TPU v7x, 32 devices: a whole 2x2x4 slice. The times are simulated.
32 devices in a mesh: sp: 8 (over z, x), tp: 4 (over y, core).
Axes of the slice: x: 2, y: 2, z: 4, core: 2. Of those that a mesh axis runs over, the one named last changes fastest.
Arguments:
- mid: bfloat16 [1536, 2048], P('sp'), may hold values from -6 to 6
- out_grad: bfloat16 [1536, 2048], P('sp'), may hold values from -6 to 6
- expert_ids: int32 [1536, 2], P('sp'), may hold values from 0 to 7, all different within a row; in each aligned block of 192 rows (0 to 191, 192 to 383, ...) at most 72 rows name the same one
- route_weights: float32 [1536, 2], P('sp'), may hold values from 0.1 to 0.9
- gate_proj: bfloat16 [8, 2048, 1024], P('sp', None, 'tp'), may hold values from -0.375 to 0.375
- up_proj: bfloat16 [8, 2048, 1024], P('sp', None, 'tp'), may hold values from -0.375 to 0.375
- down_proj: bfloat16 [8, 1024, 2048], P('sp', 'tp'), may hold values from -0.1875 to 0.1875
- out_proj: bfloat16 [512, 2048], P('tp'), may hold values from -0.25 to 0.25
- branch_gate: bfloat16 [1536, 512], P('sp', 'tp'), may hold values from -6 to 6
- conv_out: bfloat16 [2, 1536, 512], P(None, 'sp', 'tp'), may hold values from -6 to 6
- prior_state: float32 [2, 1536, 512], P(None, 'sp', 'tp'), may hold values from -6 to 6
- rate_gate_w: bfloat16 [2, 8, 64, 64], P(None, 'tp'), may hold values from -0.75 to 0.75
- input_gate_w: bfloat16 [2, 8, 64, 64], P(None, 'tp'), may hold values from -0.75 to 0.75
- decay_param: float32 [2, 512], P(None, 'tp'), may hold values from 4 to 16
- decay_jump: float32 [2, 1536, 512], P(None, 'sp', 'tp'), may hold values from -2 to 0
- conv_taps: bfloat16 [2, 4, 512], P(None, None, 'tp'), may hold values from -3 to 3
Outputs:
- gate_grad: bfloat16 [8, 2048, 1024], P('sp', None, 'tp')
- up_grad: bfloat16 [8, 2048, 1024], P('sp', None, 'tp')
- down_grad: bfloat16 [8, 1024, 2048], P('sp', 'tp')
- proj_grad_t: float32 [2048, 512], P('sp', 'tp')
- input_grad: bfloat16 [1536, 512], P('sp', 'tp')
- branch_gate_grad: bfloat16 [1536, 512], P('sp', 'tp')
Inputs may be any that keep to these rules, and one draw needn't show every extreme that they name: `expert_ids`: each row names 2 different experts. Among the rows of one device no expert is named by more than 72 rows, a bound that some block reaches of some device.
All inputs are finite; a program needn't handle non-finite values.
Results may differ from a plain program's by a relative error of at most 0.023.
The roundings to bfloat16 on the way count: a program that leaves them out, or rounds other values in their place, can miss the bound.
Values may be sent and summed in bfloat16 or wider, within the bound.
A program may use at most 64 MiB of HBM per device.

v0:
```python
import jax
import jax.numpy as jnp
from jax import lax
from jax.sharding import PartitionSpec as P

RATE_SCALE = 8.0
CLAMP_LIMIT = 7.0
SHARPNESS = 1.702
NORM_EPSILON = 1e-06
STATE_FLOOR = 0.001
GELU_CUBIC = 0.044715
GELU_SCALE = 0.7978845608028654


def carried_in(x, axis, combine, identity, reverse):
    count, place = (lax.axis_size(axis), lax.axis_index(axis))
    everything = jax.tree.map(lambda part: lax.all_gather(part, axis), x)
    start = jax.tree.map(
        lambda part, zero: jnp.broadcast_to(jnp.asarray(zero, part.dtype), part.shape), x, identity
    )

    def turn(k, before):
        at = count - 1 - k if reverse else k
        reached = at > place if reverse else at < place
        new = combine(before, jax.tree.map(lambda part: part[at], everything))
        return jax.tree.map(lambda a, b: jnp.where(reached, a, b), new, before)

    return lax.fori_loop(0, count, turn, start)


def shortened(x):
    return jax.tree.map(lambda a: a.astype(jnp.bfloat16) if a.dtype == jnp.float32 else a, x)


def with_halo(block, sides, width):
    for axis, dim in sides:
        count = lax.axis_size(axis)
        forward = [(i, i + 1) for i in range(count - 1)]
        backward = [(target, source) for source, target in forward]
        low = lax.ppermute(
            lax.slice_in_dim(block, block.shape[dim] - width, None, axis=dim), axis, forward
        )
        high = lax.ppermute(lax.slice_in_dim(block, 0, width, axis=dim), axis, backward)
        block = jnp.concatenate([low, block, high], axis=dim)
    return block


def gelu_parts(values):
    inside = GELU_SCALE * (values + GELU_CUBIC * values * values * values)
    tangent = jnp.tanh(inside)
    result = 0.5 * values * (1.0 + tangent)
    slope_value = 0.5 * (1.0 + tangent) + 0.5 * values * (1.0 - tangent * tangent) * GELU_SCALE * (
        1.0 + 3.0 * GELU_CUBIC * values * values
    )
    return (result, slope_value)


def chain_scan(factors, seeds):

    def link_pairs(first_pair, second_pair):
        return (first_pair[0] * second_pair[0], second_pair[0] * first_pair[1] + second_pair[1])

    return lax.associative_scan(link_pairs, (factors, seeds), axis=0)


def compose(former, latter):
    return (latter[0] * former[0], latter[0] * former[1] + latter[1])


def on_device(
    mid,
    out_grad,
    expert_ids,
    route_weights,
    gate_proj,
    up_proj,
    down_proj,
    out_proj,
    branch_gate,
    conv_out,
    prior_state,
    rate_gate_w,
    input_gate_w,
    decay_param,
    decay_jump,
    conv_taps,
):
    tok_rows, embedding_width = mid.shape
    shards = lax.axis_size("sp")
    groups = lax.axis_size("tp")
    local_experts = gate_proj.shape[0]
    experts_all = local_experts * shards
    top_count = expert_ids.shape[1]
    expert_room = 3 * top_count * tok_rows // (2 * experts_all)
    slot_count = experts_all * expert_room
    mid_full = mid.astype(jnp.float32)
    inv_rms = lax.rsqrt(jnp.mean(mid_full * mid_full, axis=1, keepdims=True) + NORM_EPSILON)
    normed = mid_full * inv_rms
    normed_b = normed.astype(jnp.bfloat16)
    flat_ids = expert_ids.reshape(-1)
    onehot = (flat_ids[:, None] == jnp.arange(experts_all, dtype=jnp.int32)[None, :]).astype(
        jnp.int32
    )
    rank_ids = jnp.sum((jnp.cumsum(onehot, axis=0) - onehot) * onehot, axis=1)
    slot_ids = (flat_ids * expert_room + rank_ids).reshape(tok_rows, top_count)
    matches = slot_ids[None, :, :] == jnp.arange(slot_count, dtype=jnp.int32)[:, None, None]
    select = jnp.any(matches, axis=2).astype(jnp.bfloat16)
    slot_gate = jnp.sum(jnp.where(matches, route_weights[None, :, :], 0.0), axis=(1, 2))
    column_span = embedding_width // groups
    offset = lax.axis_index("tp") * column_span
    rows_source = lax.dynamic_slice_in_dim(normed_b, offset, column_span, 1)
    grad_source = lax.dynamic_slice_in_dim(out_grad, offset, column_span, 1)
    sent_rows = jnp.dot(select, rows_source, preferred_element_type=jnp.float32).astype(
        jnp.bfloat16
    )
    dispatched_cotangent = (
        jnp.dot(select, grad_source, preferred_element_type=jnp.float32) * slot_gate[:, None]
    ).astype(jnp.bfloat16)
    got_rows, got_grad = (
        lax.all_to_all(sent_rows, "sp", split_axis=0, concat_axis=0, tiled=True),
        lax.all_to_all(dispatched_cotangent, "sp", split_axis=0, concat_axis=0, tiled=True),
    )
    got_rows, got_grad = (
        lax.all_gather(got_rows, "tp", axis=1, tiled=True),
        lax.all_gather(got_grad, "tp", axis=1, tiled=True),
    )
    expert_rows = jnp.swapaxes(
        got_rows.reshape(shards, local_experts, expert_room, embedding_width), 0, 1
    ).reshape(local_experts, shards * expert_room, embedding_width)
    expert_grads = jnp.swapaxes(
        got_grad.reshape(shards, local_experts, expert_room, embedding_width), 0, 1
    ).reshape(local_experts, shards * expert_room, embedding_width)
    gate_pre = jnp.einsum(
        "erd,edf->erf", expert_rows, gate_proj, preferred_element_type=jnp.float32
    )
    up_pre = jnp.einsum("erd,edf->erf", expert_rows, up_proj, preferred_element_type=jnp.float32)
    gate_clamped = jnp.minimum(gate_pre, CLAMP_LIMIT)
    up_clamped = jnp.clip(up_pre, -CLAMP_LIMIT, CLAMP_LIMIT)
    gate_sigmoid = jax.nn.sigmoid(SHARPNESS * gate_clamped)
    swish_value = gate_clamped * gate_sigmoid
    act_b = ((up_clamped + 1.0) * swish_value).astype(jnp.bfloat16)
    act_grad = jnp.einsum(
        "erd,efd->erf", expert_grads, down_proj, preferred_element_type=jnp.float32
    )
    gate_delta = jnp.where(
        gate_pre < CLAMP_LIMIT,
        act_grad
        * (up_clamped + 1.0)
        * (gate_sigmoid + SHARPNESS * swish_value * (1.0 - gate_sigmoid)),
        0.0,
    ).astype(jnp.bfloat16)
    up_delta = jnp.where(jnp.abs(up_pre) < CLAMP_LIMIT, act_grad * swish_value, 0.0).astype(
        jnp.bfloat16
    )
    down_grad = jnp.einsum(
        "erf,erd->efd", act_b, expert_grads, preferred_element_type=jnp.float32
    ).astype(jnp.bfloat16)
    gate_grad = jnp.einsum(
        "erd,erf->edf", expert_rows, gate_delta, preferred_element_type=jnp.float32
    ).astype(jnp.bfloat16)
    up_grad = jnp.einsum(
        "erd,erf->edf", expert_rows, up_delta, preferred_element_type=jnp.float32
    ).astype(jnp.bfloat16)
    partial_value = jnp.einsum(
        "erf,edf->erd", gate_delta, gate_proj, preferred_element_type=jnp.float32
    )
    partial_value = partial_value + jnp.einsum(
        "erf,edf->erd", up_delta, up_proj, preferred_element_type=jnp.float32
    )
    partial_rows = jnp.swapaxes(
        partial_value.reshape(local_experts, shards, expert_room, embedding_width), 0, 1
    ).reshape(slot_count, embedding_width)
    summed = lax.psum_scatter(
        partial_rows.astype(jnp.bfloat16), "tp", scatter_dimension=1, tiled=True
    )
    returned = lax.all_to_all(summed, "sp", split_axis=0, concat_axis=0, tiled=True)
    token_grad = jnp.einsum("st,sd->td", select, returned, preferred_element_type=jnp.float32)
    token_grad = lax.all_gather(token_grad.astype(jnp.bfloat16), "tp", axis=1, tiled=True).astype(
        token_grad.dtype
    )
    inner_mean = jnp.mean(token_grad * normed, axis=1, keepdims=True)
    mid_grad_b = (
        out_grad.astype(jnp.float32) + inv_rms * (token_grad - normed * inner_mean)
    ).astype(jnp.bfloat16)
    heads_local = rate_gate_w.shape[1]
    head_width = rate_gate_w.shape[2]
    channels = heads_local * head_width
    branch_grad = jnp.einsum("td,cd->tc", mid_grad_b, out_proj, preferred_element_type=jnp.float32)
    conv_heads = conv_out.reshape(2, tok_rows, heads_local, head_width)
    rate_gate = jax.nn.sigmoid(
        jnp.einsum(
            "sthc,shcd->sthd", conv_heads, rate_gate_w, preferred_element_type=jnp.float32
        ).reshape(2, tok_rows, channels)
    )
    input_gate = jax.nn.sigmoid(
        jnp.einsum(
            "sthc,shcd->sthd", conv_heads, input_gate_w, preferred_element_type=jnp.float32
        ).reshape(2, tok_rows, channels)
    )
    decay_rate = jax.nn.softplus(-decay_param)[:, None, :]
    log_decay = -RATE_SCALE * rate_gate * decay_rate + decay_jump
    decay_factors = jnp.exp(log_decay)
    squared = jnp.exp(2.0 * log_decay)
    norm_factor = jnp.sqrt(STATE_FLOOR - jnp.expm1(2.0 * log_decay))
    conv_full = conv_out.astype(jnp.float32)
    drive_term = input_gate * conv_full
    states = decay_factors * prior_state + norm_factor * drive_term
    summed_states = states[0] + states[1]
    gelu_value, gelu_slope = gelu_parts(branch_gate.astype(jnp.float32))
    mixed_b = (summed_states * gelu_value).astype(jnp.bfloat16)
    branch_gate_grad = (branch_grad * summed_states * gelu_slope).astype(jnp.bfloat16)
    state_grad = branch_grad * gelu_value
    ones_row = jnp.ones((1, channels), jnp.float32)
    later_factors = jnp.concatenate([decay_factors[0, 1:], ones_row], axis=0)
    later_prod, later_local = chain_scan(jnp.flip(later_factors, 0), jnp.flip(state_grad, 0))
    later_prod = jnp.flip(later_prod, 0)
    later_local = jnp.flip(later_local, 0)
    earlier_factors = jnp.concatenate([ones_row, decay_factors[1, :-1]], axis=0)
    earlier_prod, earlier_local = chain_scan(earlier_factors, state_grad)
    later_map = (decay_factors[0, 0] * later_prod[0], decay_factors[0, 0] * later_local[0])
    earlier_map = (
        decay_factors[1, -1] * earlier_prod[-1],
        decay_factors[1, -1] * earlier_local[-1],
    )
    identity = (jnp.ones((channels,), jnp.float32), jnp.zeros((channels,), jnp.float32))
    inflow_later = carried_in(later_map, "sp", compose, identity, True)[1]
    inflow_earlier = carried_in(earlier_map, "sp", compose, identity, False)[1]
    adjoint = jnp.stack(
        [
            later_local + later_prod * inflow_later[None, :],
            earlier_local + earlier_prod * inflow_earlier[None, :],
        ]
    )
    decay_grad = adjoint * (decay_factors * prior_state - drive_term * squared / norm_factor)
    drive_grad = adjoint * norm_factor
    rate_pre = (decay_grad * (-RATE_SCALE * decay_rate) * rate_gate * (1.0 - rate_gate)).astype(
        jnp.bfloat16
    )
    input_pre = (drive_grad * conv_full * input_gate * (1.0 - input_gate)).astype(jnp.bfloat16)
    conv_grad = drive_grad * input_gate
    conv_grad = conv_grad + jnp.einsum(
        "sthd,shcd->sthc",
        rate_pre.reshape(2, tok_rows, heads_local, head_width),
        rate_gate_w,
        preferred_element_type=jnp.float32,
    ).reshape(2, tok_rows, channels)
    conv_grad = conv_grad + jnp.einsum(
        "sthd,shcd->sthc",
        input_pre.reshape(2, tok_rows, heads_local, head_width),
        input_gate_w,
        preferred_element_type=jnp.float32,
    ).reshape(2, tok_rows, channels)
    reach = conv_taps.shape[1] - 1
    padded = with_halo(shortened(conv_grad), (("sp", 1),), reach).astype(conv_grad.dtype)
    taps_full = conv_taps.astype(jnp.float32)
    input_grad = jnp.zeros((tok_rows, channels), jnp.float32)
    for tap_index in range(reach + 1):
        upper = 2 * reach - tap_index
        input_grad = (
            input_grad
            + taps_full[0, tap_index] * padded[0, upper : upper + tok_rows]
            + taps_full[1, tap_index] * padded[1, tap_index : tap_index + tok_rows]
        )
    proj_grad_t = lax.psum_scatter(
        jnp.einsum("td,tc->dc", mid_grad_b, mixed_b, preferred_element_type=jnp.float32),
        "sp",
        scatter_dimension=0,
        tiled=True,
    )
    return (
        gate_grad,
        up_grad,
        down_grad,
        proj_grad_t,
        input_grad.astype(jnp.bfloat16),
        branch_gate_grad,
    )


def solution(mesh):
    in_specs = (
        P("sp", None),
        P("sp", None),
        P("sp", None),
        P("sp", None),
        P("sp", None, "tp"),
        P("sp", None, "tp"),
        P("sp", "tp", None),
        P("tp", None),
        P("sp", "tp"),
        P(None, "sp", "tp"),
        P(None, "sp", "tp"),
        P(None, "tp", None, None),
        P(None, "tp", None, None),
        P(None, "tp"),
        P(None, "sp", "tp"),
        P(None, None, "tp"),
    )
    out_specs = (
        P("sp", None, "tp"),
        P("sp", None, "tp"),
        P("sp", "tp", None),
        P("sp", "tp"),
        P("sp", "tp"),
        P("sp", "tp"),
    )
    return jax.shard_map(
        on_device, mesh=mesh, in_specs=in_specs, out_specs=out_specs, check_vma=False
    )
```

profile of v0, /device:TPU:0, one launch (start us, length us, event | category | flops | bytes accessed | tf_op | source)
XLA Modules:
  0.0 348.0 jit_solution(15769363398023842649)
XLA Ops:
  7.2 0.9 copy.96
  8.4 0.9 reduce-window.6
  9.9 0.7 multiply_add_fusion.16
  10.7 1.4 fusion.3
  12.1 1.3 convert_multiply_fusion.1
  13.9 23.8 %all_to_all.36 = bf16[8,72,512]{2,1,0:T(8,128)(2,1)} all-to-all(bf16[8,72,512]{2,1,0:T(8,128)(2,1)S(1)} %bitcast.219), channel_id=1, replica_groups=mesh['sp'=8,'tp'=4] {'sp'}, dimensions={0} | all-to-all | bytes 1179648 | tf_op jit(solution)/shard_map/all_to_all | solution.py:120
  38.0 1.3 fusion.8
  39.3 19.3 %all_to_all.37 = bf16[8,72,512]{2,1,0:T(8,128)(2,1)} all-to-all(bf16[8,72,512]{2,1,0:T(8,128)(2,1)S(1)} %bitcast.223), channel_id=1, replica_groups=mesh['sp'=8,'tp'=4] {'sp'}, dimensions={0} | all-to-all | bytes 1179648 | tf_op jit(solution)/shard_map/all_to_all | solution.py:121
  58.7 1.7 all-gather.7.cloned.1.call-done
  60.4 2.6 fusion.16
  63.0 1.6 fusion.22
  64.6 21.4 %all-gather.9.cloned.1.call-done = bf16[576,2048]{1,0:T(8,128)(2,1)} async-done(((bf16[576,512]{1,0:T(8,128)(2,1)}), bf16[576,2048]{1,0:T(8,128)(2,1)}) %all-gather.9.cloned.1.call-update) | async-done | bytes 2359312 | tf_op jit(solution)/shard_map/all_gather | solution.py:125
  86.0 3.2 select_convert_fusion
  89.2 0.8 fusion.20
  90.0 2.2 add_convert_fusion
  92.3 0.9 copy-done.6
  93.7 31.5 %reduce-scatter.3.cloned.1.call-done = bf16[576,512]{1,0:T(8,128)(2,1)} async-done(((bf16[576,2048]{1,0:T(8,128)(2,1)}), bf16[576,512]{1,0:T(8,128)(2,1)}) %reduce-scatter.3.cloned.1.call-update) | async-done | bytes 589840 | tf_op jit(solution)/shard_map/reduce_scatter | solution.py:173
  125.2 5.6 %all-to-all-start.2 = ((bf16[8,72,512]{2,1,0:T(8,128)(2,1)}), bf16[8,72,512]{2,1,0:T(8,128)(2,1)}, u32[]{:S(2)}, u32[]{:S(2)}) async-start(bf16[8,72,512]{2,1,0:T(8,128)(2,1)} %bitcast.222), calls=%async_computation.3 | async-start | bytes 1179648 | tf_op jit(solution)/shard_map/all_to_all | solution.py:176
  134.7 3.7 %fusion = bf16[1,2048,256]{2,1,0:T(8,128)(2,1)} fusion(bf16[576,2048]{1,0:T(8,128)(2,1)} %all-gather.7.cloned.1.call-done, bf16[576,256]{1,0:T(8,128)(2,1)S(1)} %get-tuple-element.301), kind=kOutput, calls=%fused_computation.12 | convolution fusion | flops 604504064 | bytes 3702784 | tf_op jit(solution)/shard_map/erd,erf->edf/dot_general | solution.py:158
  138.4 8.3 %all-to-all-done.2 = bf16[8,72,512]{2,1,0:T(8,128)(2,1)} async-done(((bf16[8,72,512]{2,1,0:T(8,128)(2,1)}), bf16[8,72,512]{2,1,0:T(8,128)(2,1)}, u32[]{:S(2)}, u32[]{:S(2)}) %all-to-all-start.2) | async-done | bytes 589856 | tf_op jit(solution)/shard_map/all_to_all | solution.py:176
  146.7 1.5 convolution_convert_fusion.4
  148.1 7.8 %all_gather.27 = bf16[192,2048]{1,0:T(8,128)(2,1)S(1)} all-gather(bf16[192,512]{1,0:T(8,128)(2,1)S(1)} %convolution_convert_fusion.4), channel_id=1, replica_groups=mesh['sp'=8,'tp'=4] {'tp'}, dimensions={1}, use_global_device_ids=true | all-gather | bytes 983040 | tf_op jit(solution)/shard_map/all_gather | solution.py:178
  156.4 1.2 fusion.7
  157.6 1.0 fusion.60
  158.7 0.8 multiply_add_fusion.2
  172.0 0.7 slice_multiply_fusion.3
  173.3 0.7 pad_maximum_fusion.19
  174.0 0.7 pad_maximum_fusion.16
  174.7 0.7 pad_maximum_fusion.15
  175.4 0.7 add_multiply_fusion.14
  178.8 0.8 add_multiply_fusion.6
  182.2 0.8 pad.203
  183.7 0.8 pad.202
  185.8 19.3 %all-gather.2 = f32[8,1,128]{2,1,0:T(1,128)S(1)} all-gather(f32[1,1,128]{2,1,0:T(1,128)S(1)} %get-tuple-element.308), channel_id=1, replica_groups=mesh['sp'=8,'tp'=4] {'sp'}, dimensions={0}, use_global_device_ids=true | all-gather | bytes 4608 | tf_op jit(solution)/shard_map/all_gather | solution.py:17
  205.1 16.3 %all-gather.3 = f32[8,1,128]{2,1,0:T(1,128)S(1)} all-gather(f32[1,1,128]{2,1,0:T(1,128)S(1)} %get-tuple-element.306), channel_id=1, replica_groups=mesh['sp'=8,'tp'=4] {'sp'}, dimensions={0}, use_global_device_ids=true | all-gather | bytes 4608 | tf_op jit(solution)/shard_map/all_gather | solution.py:17
  221.4 8.0 %while.31 = (s32[]{:T(128)}, f32[128]{0:T(128)}, s32[]{:T(128)}, f32[8,128]{1,0:T(8,128)S(1)}, f32[8,128]{1,0:T(8,128)S(1)}, /*index=5*/s32[]{:T(128)}, s32[]{:T(128)}) while((s32[]{:T(128)}, f32[128]{0:T(128)}, s32[]{:T(128)}, f32[8,128]{1,0:T(8,128)S(1)}, f32[8,128]{1,0:T(8,128)S(1)}, /*index=5*/s32[]{:T(128)}, ...), condition=%wide.region_12.13_spmd.clone, body=%wide.region_11.12_spmd.clone.sunk | while | flops 516 | bytes 2157 | solution.py:28
  221.9 1.1 broadcast_select_fusion.7
  223.0 1.1 broadcast_select_fusion.7
  224.0 1.1 broadcast_select_fusion.7
  225.1 1.1 broadcast_select_fusion.7
  226.2 1.1 broadcast_select_fusion.7
  227.2 1.1 broadcast_select_fusion.7
  228.3 1.1 broadcast_select_fusion.7
  230.0 1.0 rev.9
  230.9 1.0 rev.10
  231.9 18.3 %all-gather = f32[8,1,128]{2,1,0:T(1,128)S(1)} all-gather(f32[1,1,128]{2,1,0:T(1,128)S(1)} %get-tuple-element.307), channel_id=1, replica_groups=mesh['sp'=8,'tp'=4] {'sp'}, dimensions={0}, use_global_device_ids=true | all-gather | bytes 4608 | tf_op jit(solution)/shard_map/all_gather | solution.py:17
  250.2 16.3 %all-gather.1 = f32[8,1,128]{2,1,0:T(1,128)S(1)} all-gather(f32[1,1,128]{2,1,0:T(1,128)S(1)} %get-tuple-element.305), channel_id=1, replica_groups=mesh['sp'=8,'tp'=4] {'sp'}, dimensions={0}, use_global_device_ids=true | all-gather | bytes 4608 | tf_op jit(solution)/shard_map/all_gather | solution.py:17
  266.4 9.3 %while.30 = (s32[]{:T(128)}, f32[128]{0:T(128)}, s32[]{:T(128)}, f32[8,128]{1,0:T(8,128)S(1)}, f32[8,128]{1,0:T(8,128)S(1)}, /*index=5*/s32[]{:T(128)}, s32[]{:T(128)}, s32[]{:T(128)}, s32[]{:T(128)}) while((s32[]{:T(128)}, f32[128]{0:T(128)}, s32[]{:T(128)}, f32[8,128]{1,0:T(8,128)S(1)}, f32[8,128]{1,0:T(8,128)S(1)}, ...), condition=%wide.region_10.11_spmd.clone, body=%wide.region_9.10_spmd.clone.sunk | while | flops 520 | bytes 2219 | solution.py:28
  267.0 1.2 broadcast_select_fusion.6
  268.3 1.2 broadcast_select_fusion.6
  269.5 1.2 broadcast_select_fusion.6
  270.7 1.2 broadcast_select_fusion.6
  272.0 1.2 broadcast_select_fusion.6
  273.2 1.2 broadcast_select_fusion.6
  274.5 1.2 broadcast_select_fusion.6
  276.4 1.2 multiply_convert_fusion.2
  277.7 1.5 fusion.61
  279.2 3.8 %fusion.1 = bf16[1,2048,256]{2,1,0:T(8,128)(2,1)} fusion(bf16[576,2048]{1,0:T(8,128)(2,1)} %all-gather.7.cloned.1.call-done, bf16[576,256]{1,0:T(8,128)(2,1)} %copy-done.8), kind=kOutput, calls=%fused_computation.13 | convolution fusion | flops 604504064 | bytes 3702784 | tf_op jit(solution)/shard_map/erd,erf->edf/dot_general | solution.py:161
  283.1 2.1 fusion.2
  286.3 1.3 collective-permute-start.1
  287.6 4.5 %collective-permute-start = (bf16[2,3,128]{2,1,0:T(4,128)(2,1)S(1)}, bf16[2,3,128]{2,1,0:T(4,128)(2,1)S(1)}, u32[]{:S(2)}, u32[]{:S(2)}) collective-permute-start(bf16[2,3,128]{2,1,0:T(4,128)(2,1)S(1)} %get-tuple-element.311), channel_id=1, source_target_pairs={{0,4},{4,8},{8,12},{12,16},{16,20},{20,24},{24,28},{1,5},{5,9},{9,... | collective-permute-start | bytes 4616 | tf_op jit(solution)/shard_map/ppermute | solution.py:40
  292.1 0.7 fusion.39
  293.5 0.7 fusion.45
  294.2 47.2 %reduce-scatter.5.cloned.1.call-done = f32[256,128]{1,0:T(8,128)} async-done(((f32[2048,128]{1,0:T(8,128)}), f32[256,128]{1,0:T(8,128)}) %reduce-scatter.5.cloned.1.call-update) | async-done | bytes 131088 | tf_op jit(solution)/shard_map/reduce_scatter | solution.py:264
  (345 shorter events, 30.1 us)
Async XLA Ops:
  7.2 55.8 %copy-start = (bf16[1,2048,256]{2,1,0:T(8,128)(2,1)S(1)}, bf16[1,2048,256]{2,1,0:T(8,128)(2,1)}, u32[]{:S(2)}) copy-start(bf16[1,2048,256]{2,1,0:T(8,128)(2,1)} %param.24) | copy-start | bytes 3145732
  7.2 53.2 %all-gather.7.cloned.1.call-start = ((), (), s32[]{:S(2)}) async-start(), calls=%async_computation.5 | async-start | bytes 2949120 | tf_op jit(solution)/shard_map/all_gather | solution.py:124
  10.7 27.1 %copy-start.31 = (f32[192,2]{0,1:T(2,128)S(1)}, f32[192,2]{0,1:T(2,128)}, u32[]{:S(2)}) copy-start(f32[192,2]{0,1:T(2,128)} %param.23) | copy-start | bytes 4612
  12.1 143.9 %copy-start.16 = (f32[192]{0:T(256)}, f32[192]{0:T(256)S(1)}, u32[]{:S(2)}) copy-start(f32[192]{0:T(256)S(1)} %add_rsqrt_fusion) | copy-start | bytes 2308
  13.8 46.5 %copy-start.2 = (bf16[1,2048,256]{2,1,0:T(8,128)(2,1)S(1)}, bf16[1,2048,256]{2,1,0:T(8,128)(2,1)}, u32[]{:S(2)}) copy-start(bf16[1,2048,256]{2,1,0:T(8,128)(2,1)} %param.25) | copy-start | bytes 3145732
  37.7 48.3 %all-gather.9.cloned.1.call-start = ((), (), s32[]{:S(2)}) async-start(), calls=%async_computation.6 | async-start | bytes 2949120 | tf_op jit(solution)/shard_map/all_gather | solution.py:125
  58.7 66.5 %reduce-scatter.3.cloned.1.call-start = ((), (), s32[]{:S(2)}) async-start(), calls=%async_computation.7 | async-start | bytes 2949120 | tf_op jit(solution)/shard_map/reduce_scatter | solution.py:173
  60.4 2.6 copy-start.33
  63.0 23.0 %copy-start.35 = (f32[576,256]{1,0:T(8,128)}, f32[576,256]{1,0:T(8,128)S(1)}, u32[]{:S(2)}) copy-start(f32[576,256]{1,0:T(8,128)S(1)} %fusion.16) | copy-start | bytes 1769476
  89.2 0.8 copy-start.8
  92.2 0.9 copy-start.6
  92.2 1.0 copy-start.14
  92.2 1.4 copy-start.32
  92.2 38.6 %copy-start.11 = (f32[2,192,128]{2,1,0:T(8,128)S(1)}, f32[2,192,128]{2,1,0:T(8,128)}, u32[]{:S(2)}) copy-start(f32[2,192,128]{2,1,0:T(8,128)} %param.34) | copy-start | bytes 589828
  93.3 40.4 %copy-start.12 = (bf16[2,2,64,64]{3,2,1,0:T(8,128)(2,1)S(1)}, bf16[2,2,64,64]{3,2,1,0:T(8,128)(2,1)}, u32[]{:S(2)}) copy-start(bf16[2,2,64,64]{3,2,1,0:T(8,128)(2,1)} %param.32) | copy-start | bytes 98308
  93.7 40.2 %copy-start.17 = (f32[2,128]{1,0:T(2,128)}, f32[2,128]{1,0:T(2,128)S(1)}, u32[]{:S(2)}) copy-start(f32[2,128]{1,0:T(2,128)S(1)} %fusion.78) | copy-start | bytes 3076
  125.2 8.9 %copy-start.30 = (bf16[2,4,128]{2,1,0:T(4,128)(2,1)S(1)}, bf16[2,4,128]{2,1,0:T(4,128)(2,1)}, u32[]{:S(2)}) copy-start(bf16[2,4,128]{2,1,0:T(4,128)(2,1)} %param.35) | copy-start | bytes 6148
  125.2 21.5 %all-to-all-start.2 = ((bf16[8,72,512]{2,1,0:T(8,128)(2,1)}), bf16[8,72,512]{2,1,0:T(8,128)(2,1)}, u32[]{:S(2)}, u32[]{:S(2)}) async-start(bf16[8,72,512]{2,1,0:T(8,128)(2,1)} %bitcast.222), calls=%async_computation.3 | async-start | bytes 1179648 | tf_op jit(solution)/shard_map/all_to_all | solution.py:176
  130.8 210.6 %reduce-scatter.5.cloned.1.call-start = ((), (), s32[]{:S(2)}) async-start(), calls=%async_computation.8 | async-start | bytes 1179648 | tf_op jit(solution)/shard_map/reduce_scatter | solution.py:264
  138.4 17.6 %copy-start.1 = (bf16[192,2048]{1,0:T(8,128)(2,1)S(1)}, bf16[192,2048]{1,0:T(8,128)(2,1)}, u32[]{:S(2)}) copy-start(bf16[192,2048]{1,0:T(8,128)(2,1)} %param.20) | copy-start | bytes 2359300
  146.7 9.7 %copy-start.3 = (bf16[192,2048]{1,0:T(8,128)(2,1)S(1)}, bf16[192,2048]{1,0:T(8,128)(2,1)}, u32[]{:S(2)}) copy-start(bf16[192,2048]{1,0:T(8,128)(2,1)} %param.21) | copy-start | bytes 2359300
  156.0 1.6 copy-start.4
  156.0 1.6 copy-start.5
  157.6 3.1 copy-start.9
  157.6 3.1 copy-start.10
  171.0 0.8 copy-start.19
  171.1 0.6 copy-start.29
  171.2 0.7 copy-start.20
  178.1 98.3 %copy-start.18 = (f32[2,128]{1,0:T(2,128)S(1)}, f32[2,128]{1,0:T(2,128)}, u32[]{:S(2)}) copy-start(f32[2,128]{1,0:T(2,128)} %copy-done.17) | copy-start | bytes 3076
  279.2 3.9 %copy-start.34 = (bf16[576,2048]{1,0:T(8,128)(2,1)S(1)}, bf16[576,2048]{1,0:T(8,128)(2,1)}, u32[]{:S(2)}) copy-start(bf16[576,2048]{1,0:T(8,128)(2,1)} %all-gather.9.cloned.1.call-done) | copy-start | bytes 7077892
  279.2 3.9 %copy-start.36 = (f32[576,256]{1,0:T(8,128)S(1)}, f32[576,256]{1,0:T(8,128)}, u32[]{:S(2)}) copy-start(f32[576,256]{1,0:T(8,128)} %copy-done.35) | copy-start | bytes 1769476
  279.2 3.9 %copy-start.37 = (f32[576,256]{1,0:T(8,128)S(1)}, f32[576,256]{1,0:T(8,128)}, u32[]{:S(2)}) copy-start(f32[576,256]{1,0:T(8,128)} %fusion.22) | copy-start | bytes 1769476
  283.0 2.3 copy-start.13
  283.1 2.7 copy-start.15
  285.2 6.9 %copy-start.7 = (f32[192,128]{1,0:T(8,128)S(1)}, f32[192,128]{1,0:T(8,128)}, u32[]{:S(2)}) copy-start(f32[192,128]{1,0:T(8,128)} %get-tuple-element.380) | copy-start | bytes 294916
  285.2 8.3 %copy-start.21 = (f32[128]{0:T(128)S(1)}, f32[128]{0:T(128)}, u32[]{:S(2)}) copy-start(f32[128]{0:T(128)} %get-tuple-element.347) | copy-start | bytes 1540
  285.2 8.3 %copy-start.22 = (f32[128]{0:T(128)S(1)}, f32[128]{0:T(128)}, u32[]{:S(2)}) copy-start(f32[128]{0:T(128)} %get-tuple-element.348) | copy-start | bytes 1540
  285.2 8.3 %copy-start.23 = (f32[128]{0:T(128)S(1)}, f32[128]{0:T(128)}, u32[]{:S(2)}) copy-start(f32[128]{0:T(128)} %get-tuple-element.349) | copy-start | bytes 1540
  285.2 8.3 %copy-start.24 = (f32[128]{0:T(128)S(1)}, f32[128]{0:T(128)}, u32[]{:S(2)}) copy-start(f32[128]{0:T(128)} %get-tuple-element.350) | copy-start | bytes 1540
  285.2 8.3 %copy-start.25 = (f32[128]{0:T(128)S(1)}, f32[128]{0:T(128)}, u32[]{:S(2)}) copy-start(f32[128]{0:T(128)} %get-tuple-element.351) | copy-start | bytes 1540
  285.2 8.3 %copy-start.26 = (f32[128]{0:T(128)S(1)}, f32[128]{0:T(128)}, u32[]{:S(2)}) copy-start(f32[128]{0:T(128)} %get-tuple-element.352) | copy-start | bytes 1540
  285.2 8.3 %copy-start.27 = (f32[128]{0:T(128)S(1)}, f32[128]{0:T(128)}, u32[]{:S(2)}) copy-start(f32[128]{0:T(128)} %get-tuple-element.353) | copy-start | bytes 1540
  285.2 8.3 %copy-start.28 = (f32[128]{0:T(128)S(1)}, f32[128]{0:T(128)}, u32[]{:S(2)}) copy-start(f32[128]{0:T(128)} %get-tuple-element.354) | copy-start | bytes 1540
  286.3 6.6 %collective-permute-start.1 = (bf16[2,3,128]{2,1,0:T(4,128)(2,1)S(1)}, bf16[2,3,128]{2,1,0:T(4,128)(2,1)S(1)}, u32[]{:S(2)}, u32[]{:S(2)}) collective-permute-start(bf16[2,3,128]{2,1,0:T(4,128)(2,1)S(1)} %get-tuple-element.312), channel_id=1, source_target_pairs={{4,0},{8,4},{12,8},{16,12},{20,16},{24,20},{28,24},{5,1},{9,5},{13... | collective-permute-start | bytes 4616 | tf_op jit(solution)/shard_map/ppermute | solution.py:43
  287.6 5.8 %collective-permute-start = (bf16[2,3,128]{2,1,0:T(4,128)(2,1)S(1)}, bf16[2,3,128]{2,1,0:T(4,128)(2,1)S(1)}, u32[]{:S(2)}, u32[]{:S(2)}) collective-permute-start(bf16[2,3,128]{2,1,0:T(4,128)(2,1)S(1)} %get-tuple-element.311), channel_id=1, source_target_pairs={{0,4},{4,8},{8,12},{12,16},{16,20},{20,24},{24,28},{1,5},{5,9},{9,... | collective-permute-start | bytes 4616 | tf_op jit(solution)/shard_map/ppermute | solution.py:40
Sparse Core Ops, SparseCore 0:
  37.8 22.4 all-gather.6
  61.9 24.0 all-gather.8
  92.4 32.7 reduce-scatter.2
  279.3 62.1 reduce-scatter.4
where the time goes:
time: 349 us; the launch traced here: 348 us
  blocking collectives  121 us (35%)
  waiting for transfers between devices  111 us (32%)
  other arithmetic  40.2 us (12%)
  matrix products  26.5 us (8%)
  local copies, waits for them, and re-layouts  22.4 us (6%)
  between operations  15.3 us (4%)
  starting transfers between devices  11.6 us (3%)
    all_gather x4, blocking collectives, carried_in(): everything = jax.tree.map(lambda part: lax.all_gather(part, axis), x)  70.1 us
    reduce_scatter x1, waiting for transfers between devices, on_device(): lax.psum_scatter(jnp.einsum('td,tc->dc', mid_grad_b, mixed_b, preferred_e...  47.2 us
    reduce_scatter x1, waiting for transfers between devices, on_device(): lax.psum_scatter(partial_rows.astype(jnp.bfloat16), 'tp', scatter_dimensi...  31.5 us
    all_to_all x1, blocking collectives, on_device(): lax.all_to_all(sent_rows, 'sp', split_axis=0, concat_axis=0, tiled=True)  23.8 us
    all_gather x1, waiting for transfers between devices, on_device(): lax.all_gather(got_grad, 'tp', axis=1, tiled=True)  21.4 us
    all_to_all x1, blocking collectives, on_device(): lax.all_to_all(dispatched_cotangent, 'sp', split_axis=0, concat_axis=0, t...  19.3 us
    select_n x16, other arithmetic, turn(): return jax.tree.map(lambda a, b: jnp.where(reached, a, b), new, before)  17.2 us
    slice x97, local copies, waits for them, and re-layouts, chain_scan(): return lax.associative_scan(link_pairs, (factors, seeds), axis=0)  13.7 us
  transfers between devices with their start and end apart: 7, of which 6 were waited for; matrix products, arithmetic and copies ran while one was open for 6% of the time, Pallas kernels for 0%

commit v1 on v0

v1 whole, which is shorter than its diff:
```python
import functools

import jax
import jax.numpy as jnp
from jax import lax
from jax.experimental import pallas as pl
from jax.experimental.pallas import tpu as pltpu
from jax.sharding import PartitionSpec as P

MESH = pl.DeviceIdType.MESH

RATE_SCALE = 8.0
CLAMP_LIMIT = 7.0
SHARPNESS = 1.702
NORM_EPSILON = 1e-06
STATE_FLOOR = 0.001
GELU_CUBIC = 0.044715
GELU_SCALE = 0.7978845608028654


def gelu_parts(values):
    inside = GELU_SCALE * (values + GELU_CUBIC * values * values * values)
    tangent = jnp.tanh(inside)
    result = 0.5 * values * (1.0 + tangent)
    slope_value = 0.5 * (1.0 + tangent) + 0.5 * values * (1.0 - tangent * tangent) * GELU_SCALE * (
        1.0 + 3.0 * GELU_CUBIC * values * values
    )
    return (result, slope_value)


def greet(n, g):
    me, t = lax.axis_index("sp"), lax.axis_index("tp")
    barrier = pltpu.get_barrier_semaphore()

    def over_sp(k, carry):
        peer = lax.rem(me + k, n)
        pl.semaphore_signal(barrier, inc=1, device_id={"sp": peer}, device_id_type=MESH)
        return carry

    def over_tp(k, carry):
        peer = lax.rem(t + k, g)
        pl.semaphore_signal(barrier, inc=1, device_id={"tp": peer}, device_id_type=MESH)
        return carry

    lax.fori_loop(1, n, over_sp, 0)
    lax.fori_loop(1, g, over_tp, 0)
    pl.semaphore_wait(barrier, n + g - 2)


def remote(src, dst, send_sem, recv_sem, axis, peer):
    return pltpu.make_async_remote_copy(
        src_ref=src, dst_ref=dst, send_sem=send_sem, recv_sem=recv_sem,
        device_id={axis: peer}, device_id_type=MESH,
    )


def front_kernel(n, g, send, got, sp_send, sp_recv, tp_send, tp_recv, own_sem):
    me, t = lax.axis_index("sp"), lax.axis_index("tp")
    low = lax.rem(t, 2)
    high = t // 2
    highs = g // 2
    partner = high * 2 + 1 - low
    width = send.shape[-1]

    def block(p, q):
        return got.at[:, p, :, pl.ds(pl.multiple_of(q * width, width), width)]

    def over_sp(p):
        return remote(send.at[:, p], block(me, t), sp_send.at[p], sp_recv.at[me], "sp", p)

    def from_sp(p):
        return remote(send.at[:, p], block(p, t), sp_send.at[p], sp_recv.at[p], "sp", p)

    def over_tp(kind, p, q, peer):
        return remote(block(p, q), block(p, q), tp_send.at[kind, p], tp_recv.at[q, p], "tp", peer)

    own = pltpu.make_async_copy(send.at[:, me], block(me, t), own_sem)
    own.start()
    greet(n, g)

    def start(k, carry):
        over_sp(lax.rem(me + k, n)).start()
        return carry

    lax.fori_loop(1, n, start, 0)
    own.wait()

    def spread(p):
        for j in range(1, highs):
            over_tp(j, p, t, lax.rem(high + j, highs) * 2 + low).start()
        over_tp(0, p, t, partner).start()

    def forward(p):
        for j in range(1, highs):
            q = lax.rem(high + highs - j, highs) * 2 + low
            over_tp(j, p, q, q).wait_recv()
            over_tp(highs - 1 + j, p, q, partner).start()

    spread(me)

    def step(k, carry):
        p = lax.rem(me + n - k, n)
        from_sp(p).wait_recv()
        spread(p)
        forward(lax.rem(p + 1, n))
        return carry

    lax.fori_loop(1, n, step, 0)
    forward(lax.rem(me + 1, n))

    def finish(k, carry):
        p = lax.rem(me + n - k, n)
        for j in range(highs):
            q = lax.rem(high + highs - j, highs) * 2 + 1 - low
            over_tp(0, p, q, partner).wait_recv()
        for kind in range(2 * highs - 1):
            over_tp(kind, p, t, partner).wait_send()
        return carry

    lax.fori_loop(0, n, finish, 0)

    def sent(k, carry):
        over_sp(lax.rem(me + k, n)).wait_send()
        return carry

    lax.fori_loop(1, n, sent, 0)


def shifted(x, by, fill, down):
    rows = x.shape[0]
    at = lax.broadcasted_iota(jnp.int32, x.shape, 0)
    if down:
        return jnp.where(at >= by, pltpu.roll(x, by, 0), fill)
    return jnp.where(at < rows - by, pltpu.roll(x, rows - by, 0), fill)


def chain_scan(factors, seeds, down):
    by = 1
    while by < seeds.shape[0]:
        seeds = seeds + factors * shifted(seeds, by, 0.0, down)
        factors = factors * shifted(factors, by, 1.0, down)
        by *= 2
    return factors, seeds


def dot_last(a, b):
    return lax.dot_general(a, b, (((1,), (1,)), ((), ())), preferred_element_type=jnp.float32)


def back_kernel(
    n, g, partial, select, mid, out_grad, out_proj, branch_gate, conv, prior, rate_w, input_w,
    rate, jump, taps, proj_o, input_o, branch_o,
    pair, held, crossed, ready, returned, total, token, midg, decay, rate_c, input_c, drive_c,
    proj, proj_send, proj_recv, carry_send, carries, padded,
    pair_send, pair_recv, high_send, high_recv, sp_send, sp_recv, tok_send, tok_recv,
    rs_send, rs_recv, map_send, map_recv, halo_send, halo_recv,
):
    me, t = lax.axis_index("sp"), lax.axis_index("tp")
    low = lax.rem(t, 2)
    high = t // 2
    highs = g // 2
    partner = high * 2 + 1 - low
    width = returned.shape[-1]
    rows, channels = branch_gate.shape
    f32 = jnp.float32

    def cols(q):
        return pl.ds(pl.multiple_of(q * width, width), width)

    def to_pair(h, p):
        return remote(
            partial.at[p, :, cols(h * 2 + 1 - low)], pair.at[h, p],
            pair_send.at[h, p], pair_recv.at[h, p], "tp", partner,
        )

    def to_high(j, p):
        return remote(
            held.at[j - 1, p], crossed.at[j - 1, p],
            high_send.at[j - 1, p], high_recv.at[j - 1, p], "tp",
            lax.rem(high + j, highs) * 2 + low,
        )

    def to_sp(p):
        return remote(ready.at[p], returned.at[me], sp_send.at[p], sp_recv.at[me], "sp", p)

    def from_sp(p):
        return remote(ready.at[p], returned.at[p], sp_send.at[p], sp_recv.at[p], "sp", p)

    greet(n, g)

    def first(k, carry):
        p = lax.rem(me + k, n)
        for j in range(1, highs + 1):
            to_pair(lax.rem(high + j, highs), p).start()
        return carry

    lax.fori_loop(1, n + 1, first, 0)

    def second(k, carry):
        p = lax.rem(me + k, n)
        for j in range(1, highs):
            h = lax.rem(high + j, highs)
            to_pair(h, p).wait_recv()
            held[j - 1, p] = (
                partial[p, :, cols(h * 2 + low)].astype(f32) + pair[h, p].astype(f32)
            ).astype(jnp.bfloat16)
            to_high(j, p).start()
        return carry

    lax.fori_loop(1, n + 1, second, 0)

    summed = jnp.zeros((rows, channels), f32)
    for side in range(2):
        taken = conv[side]
        rate_gate = jax.nn.sigmoid(jnp.dot(taken, rate_w[side], preferred_element_type=f32))
        input_gate = jax.nn.sigmoid(jnp.dot(taken, input_w[side], preferred_element_type=f32))
        speed = rate[side : side + 1, :]
        log_decay = speed * rate_gate + jump[side]
        factors = jnp.exp(log_decay)
        squared = jnp.exp(2.0 * log_decay)
        norm_factor = jnp.sqrt((1.0 + STATE_FLOOR) - squared)
        full = taken.astype(f32)
        drive = input_gate * full
        carried = factors * prior[side]
        summed = summed + carried + norm_factor * drive
        decay[side] = factors
        rate_c[side] = (
            (carried - drive * squared / norm_factor) * speed * rate_gate * (1.0 - rate_gate)
        )
        input_c[side] = norm_factor * full * input_gate * (1.0 - input_gate)
        drive_c[side] = norm_factor * input_gate
    gelu_value, gelu_slope = gelu_parts(branch_gate[...].astype(f32))
    mixed = (summed * gelu_value).astype(jnp.bfloat16)
    slope = summed * gelu_slope

    def third(k, carry):
        p = lax.rem(me + k, n)
        to_pair(high, p).wait_recv()
        value = partial[p, :, cols(t)].astype(f32) + pair[high, p].astype(f32)
        for j in range(1, highs):
            to_high(j, p).wait_recv()
            value = value + crossed[j - 1, p].astype(f32)
        ready[p] = value.astype(jnp.bfloat16)

        @pl.when(k < n)
        def _():
            to_sp(p).start()

        return carry

    lax.fori_loop(1, n + 1, third, 0)
    total[...] = jnp.dot(select[me], ready[me], preferred_element_type=f32)

    def fourth(k, carry):
        p = lax.rem(me + n - k, n)
        from_sp(p).wait_recv()
        total[...] += jnp.dot(select[p], returned[p], preferred_element_type=f32)
        return carry

    lax.fori_loop(1, n, fourth, 0)

    def share(kind, q, peer):
        return remote(
            token.at[:, cols(q)], token.at[:, cols(q)], tok_send.at[kind], tok_recv.at[q],
            "tp", peer,
        )

    token[:, cols(t)] = total[...].astype(jnp.bfloat16)
    for j in range(1, highs):
        share(j, t, lax.rem(high + j, highs) * 2 + low).start()
    share(0, t, partner).start()
    for j in range(1, highs):
        q = lax.rem(high + highs - j, highs) * 2 + low
        share(j, q, q).wait_recv()
        share(highs - 1 + j, q, partner).start()
    for j in range(highs):
        q = lax.rem(high + highs - j, highs) * 2 + 1 - low
        share(0, q, partner).wait_recv()

    piece = 16

    def normal(k, carry):
        at = pl.ds(pl.multiple_of(k * piece, piece), piece)
        values = mid[at, :].astype(f32)
        inv_rms = lax.rsqrt(jnp.mean(values * values, axis=1, keepdims=True) + NORM_EPSILON)
        normed = values * inv_rms
        grad = token[at, :].astype(f32)
        inner = jnp.mean(grad * normed, axis=1, keepdims=True)
        midg[at, :] = (
            out_grad[at, :].astype(f32) + inv_rms * (grad - normed * inner)
        ).astype(jnp.bfloat16)
        return carry

    lax.fori_loop(0, rows // piece, normal, 0)

    branch_grad = dot_last(midg[...], out_proj[...])
    branch_o[...] = (branch_grad * slope).astype(jnp.bfloat16)
    seeds = branch_grad * gelu_value
    later_prod, later_local = chain_scan(shifted(decay[0], 1, 1.0, False), seeds, False)
    earlier_prod, earlier_local = chain_scan(shifted(decay[1], 1, 1.0, True), seeds, True)
    first_decay, last_decay = decay[0, 0:1, :], decay[1, rows - 1 : rows, :]
    carry_send[0:1, :] = first_decay * later_prod[0:1]
    carry_send[1:2, :] = first_decay * later_local[0:1]
    carry_send[2:3, :] = last_decay * earlier_prod[rows - 1 : rows]
    carry_send[3:4, :] = last_decay * earlier_local[rows - 1 : rows]
    carry_send[4:8, :] = jnp.zeros((4, channels), f32)

    def to_map(p):
        return remote(carry_send, carries.at[me], map_send.at[p], map_recv.at[me], "sp", p)

    def from_map(p):
        return remote(carry_send, carries.at[p], map_send.at[p], map_recv.at[p], "sp", p)

    def maps(k, carry):
        to_map(lax.rem(me + k, n)).start()
        return carry

    lax.fori_loop(1, n, maps, 0)
    carries[me] = carry_send[...]

    product = lax.dot_general(
        midg[...], mixed, (((0,), (0,)), ((), ())), preferred_element_type=f32
    ).reshape(proj.shape)
    proj[...] = product
    proj_send[...] = product.astype(jnp.bfloat16)

    def to_rs(p):
        return remote(proj_send.at[p], proj_recv.at[me], rs_send.at[p], rs_recv.at[me], "sp", p)

    def from_rs(p):
        return remote(proj_send.at[p], proj_recv.at[p], rs_send.at[p], rs_recv.at[p], "sp", p)

    def scatter(k, carry):
        to_rs(lax.rem(me + k, n)).start()
        return carry

    lax.fori_loop(1, n, scatter, 0)

    def landed(k, carry):
        from_map(lax.rem(me + n - k, n)).wait_recv()
        return carry

    lax.fori_loop(1, n, landed, 0)

    def flow(k, carry):
        later, earlier = carry
        j = n - 1 - k
        later = jnp.where(j > me, carries[j, 0:1, :] * later + carries[j, 1:2, :], later)
        earlier = jnp.where(k < me, carries[k, 2:3, :] * earlier + carries[k, 3:4, :], earlier)
        return later, earlier

    nothing = jnp.zeros((1, channels), f32)
    later_in, earlier_in = lax.fori_loop(0, n, flow, (nothing, nothing))
    adjoints = (later_local + later_prod * later_in, earlier_local + earlier_prod * earlier_in)
    edge = 8
    for side in range(2):
        adjoint = adjoints[side]
        rate_pre = (adjoint * rate_c[side]).astype(jnp.bfloat16)
        input_pre = (adjoint * input_c[side]).astype(jnp.bfloat16)
        padded[side, edge : edge + rows, :] = (
            adjoint * drive_c[side]
            + dot_last(rate_pre, rate_w[side])
            + dot_last(input_pre, input_w[side])
        )
    after, before = lax.rem(me + 1, n), lax.rem(me + n - 1, n)
    up = remote(
        padded.at[:, pl.ds(rows, edge)], padded.at[:, pl.ds(0, edge)],
        halo_send.at[0], halo_recv.at[0], "sp", after,
    )
    down = remote(
        padded.at[:, pl.ds(edge, edge)], padded.at[:, pl.ds(edge + rows, edge)],
        halo_send.at[1], halo_recv.at[1], "sp", before,
    )
    up.start()
    down.start()
    up.wait()
    down.wait()
    reach = taps.shape[1] - 1
    front = jnp.where(me > 0, padded[:, 0:edge, :], 0.0)
    end = jnp.where(me < n - 1, padded[:, edge + rows : 2 * edge + rows, :], 0.0)
    padded[:, 0:edge, :] = front
    padded[:, edge + rows : 2 * edge + rows, :] = end
    result = jnp.zeros((rows, channels), f32)
    for k in range(reach + 1):
        result = (
            result
            + taps[0, k : k + 1, :] * padded[0, edge + reach - k : edge + reach - k + rows, :]
            + taps[1, k : k + 1, :] * padded[1, edge - reach + k : edge - reach + k + rows, :]
        )
    input_o[...] = result.astype(jnp.bfloat16)

    proj_o[...] = proj[me]

    def gather(k, carry):
        p = lax.rem(me + n - k, n)
        from_rs(p).wait_recv()
        proj_o[...] += proj_recv[p].astype(f32)
        return carry

    lax.fori_loop(1, n, gather, 0)

    def sent(k, carry):
        p = lax.rem(me + k, n)
        to_sp(p).wait_send()
        to_map(p).wait_send()
        to_rs(p).wait_send()
        return carry

    lax.fori_loop(1, n, sent, 0)

    def sent_tp(p, carry):
        for h in range(highs):
            to_pair(h, p).wait_send()
        for j in range(1, highs):
            to_high(j, p).wait_send()
        return carry

    lax.fori_loop(0, n, sent_tp, 0)
    for kind in range(2 * highs - 1):
        share(kind, t, partner).wait_send()


def on_device(
    mid,
    out_grad,
    expert_ids,
    route_weights,
    gate_proj,
    up_proj,
    down_proj,
    out_proj,
    branch_gate,
    conv_out,
    prior_state,
    rate_gate_w,
    input_gate_w,
    decay_param,
    decay_jump,
    conv_taps,
):
    tok_rows, embedding_width = mid.shape
    shards = lax.axis_size("sp")
    groups = lax.axis_size("tp")
    local_experts = gate_proj.shape[0]
    experts_all = local_experts * shards
    top_count = expert_ids.shape[1]
    expert_room = 3 * top_count * tok_rows // (2 * experts_all)
    slot_count = experts_all * expert_room
    mid_full = mid.astype(jnp.float32)
    inv_rms = lax.rsqrt(jnp.mean(mid_full * mid_full, axis=1, keepdims=True) + NORM_EPSILON)
    normed = mid_full * inv_rms
    normed_b = normed.astype(jnp.bfloat16)
    flat_ids = expert_ids.reshape(-1)
    onehot = (flat_ids[:, None] == jnp.arange(experts_all, dtype=jnp.int32)[None, :]).astype(
        jnp.int32
    )
    rank_ids = jnp.sum((jnp.cumsum(onehot, axis=0) - onehot) * onehot, axis=1)
    slot_ids = (flat_ids * expert_room + rank_ids).reshape(tok_rows, top_count)
    matches = slot_ids[None, :, :] == jnp.arange(slot_count, dtype=jnp.int32)[:, None, None]
    select = jnp.any(matches, axis=2).astype(jnp.bfloat16)
    slot_gate = jnp.sum(jnp.where(matches, route_weights[None, :, :], 0.0), axis=(1, 2))
    column_span = embedding_width // groups
    offset = lax.axis_index("tp") * column_span
    rows_source = lax.dynamic_slice_in_dim(normed_b, offset, column_span, 1)
    grad_source = lax.dynamic_slice_in_dim(out_grad, offset, column_span, 1)
    sent_rows = jnp.dot(select, rows_source, preferred_element_type=jnp.float32).astype(
        jnp.bfloat16
    )
    dispatched_cotangent = (
        jnp.dot(select, grad_source, preferred_element_type=jnp.float32) * slot_gate[:, None]
    ).astype(jnp.bfloat16)
    sending = jnp.stack([sent_rows, dispatched_cotangent]).reshape(
        2, shards, local_experts * expert_room, column_span
    )
    dma = pltpu.SemaphoreType.DMA
    vmem = pl.BlockSpec(memory_space=pltpu.VMEM)
    got = pl.pallas_call(
        functools.partial(front_kernel, shards, groups),
        out_shape=jax.ShapeDtypeStruct(
            (2, shards, local_experts * expert_room, embedding_width), jnp.bfloat16
        ),
        in_specs=[vmem],
        out_specs=vmem,
        scratch_shapes=[
            dma((shards,)), dma((shards,)), dma((groups - 1, shards)), dma((groups, shards)),
            dma(()),
        ],
        compiler_params=pltpu.CompilerParams(collective_id=0, has_side_effects=True),
    )(sending)

    def by_expert(block):
        return jnp.swapaxes(
            block.reshape(shards, local_experts, expert_room, embedding_width), 0, 1
        ).reshape(local_experts, shards * expert_room, embedding_width)

    expert_rows, expert_grads = by_expert(got[0]), by_expert(got[1])
    gate_pre = jnp.einsum(
        "erd,edf->erf", expert_rows, gate_proj, preferred_element_type=jnp.float32
    )
    up_pre = jnp.einsum("erd,edf->erf", expert_rows, up_proj, preferred_element_type=jnp.float32)
    gate_clamped = jnp.minimum(gate_pre, CLAMP_LIMIT)
    up_clamped = jnp.clip(up_pre, -CLAMP_LIMIT, CLAMP_LIMIT)
    gate_sigmoid = jax.nn.sigmoid(SHARPNESS * gate_clamped)
    swish_value = gate_clamped * gate_sigmoid
    act_b = ((up_clamped + 1.0) * swish_value).astype(jnp.bfloat16)
    act_grad = jnp.einsum(
        "erd,efd->erf", expert_grads, down_proj, preferred_element_type=jnp.float32
    )
    gate_delta = jnp.where(
        gate_pre < CLAMP_LIMIT,
        act_grad
        * (up_clamped + 1.0)
        * (gate_sigmoid + SHARPNESS * swish_value * (1.0 - gate_sigmoid)),
        0.0,
    ).astype(jnp.bfloat16)
    up_delta = jnp.where(jnp.abs(up_pre) < CLAMP_LIMIT, act_grad * swish_value, 0.0).astype(
        jnp.bfloat16
    )
    down_grad = jnp.einsum(
        "erf,erd->efd", act_b, expert_grads, preferred_element_type=jnp.float32
    ).astype(jnp.bfloat16)
    gate_grad = jnp.einsum(
        "erd,erf->edf", expert_rows, gate_delta, preferred_element_type=jnp.float32
    ).astype(jnp.bfloat16)
    up_grad = jnp.einsum(
        "erd,erf->edf", expert_rows, up_delta, preferred_element_type=jnp.float32
    ).astype(jnp.bfloat16)
    partial_value = jnp.einsum(
        "erf,edf->erd", gate_delta, gate_proj, preferred_element_type=jnp.float32
    )
    partial_value = partial_value + jnp.einsum(
        "erf,edf->erd", up_delta, up_proj, preferred_element_type=jnp.float32
    )
    room = local_experts * expert_room
    partial_rows = jnp.swapaxes(
        partial_value.reshape(local_experts, shards, expert_room, embedding_width), 0, 1
    ).reshape(shards, room, embedding_width).astype(jnp.bfloat16)
    token_slots = jnp.arange(slot_count, dtype=jnp.int32).reshape(shards, 1, room)
    select_t = jnp.any(
        slot_ids[None, :, None, :] == token_slots[:, :, :, None], axis=3
    ).astype(jnp.bfloat16)
    heads_local = rate_gate_w.shape[1]
    head_width = rate_gate_w.shape[2]
    channels = heads_local * head_width
    same_head = jnp.eye(heads_local, dtype=jnp.bfloat16)[None, :, None, :, None]

    def block_diagonal(blocks):
        return (blocks[:, :, :, None, :] * same_head).reshape(2, channels, channels)

    speed = -RATE_SCALE * jax.nn.softplus(-decay_param)
    highs = groups // 2
    bf16, f32 = jnp.bfloat16, jnp.float32
    proj_rows = embedding_width // shards
    proj_grad_t, input_grad, branch_gate_grad = pl.pallas_call(
        functools.partial(back_kernel, shards, groups),
        out_shape=(
            jax.ShapeDtypeStruct((proj_rows, channels), f32),
            jax.ShapeDtypeStruct((tok_rows, channels), bf16),
            jax.ShapeDtypeStruct((tok_rows, channels), bf16),
        ),
        in_specs=[vmem] * 13,
        out_specs=(vmem,) * 3,
        scratch_shapes=[
            pltpu.VMEM((highs, shards, room, column_span), bf16),
            pltpu.VMEM((highs - 1, shards, room, column_span), bf16),
            pltpu.VMEM((highs - 1, shards, room, column_span), bf16),
            pltpu.VMEM((shards, room, column_span), bf16),
            pltpu.VMEM((shards, room, column_span), bf16),
            pltpu.VMEM((tok_rows, column_span), f32),
            pltpu.VMEM((tok_rows, embedding_width), bf16),
            pltpu.VMEM((tok_rows, embedding_width), bf16),
            pltpu.VMEM((2, tok_rows, channels), f32),
            pltpu.VMEM((2, tok_rows, channels), f32),
            pltpu.VMEM((2, tok_rows, channels), f32),
            pltpu.VMEM((2, tok_rows, channels), f32),
            pltpu.VMEM((shards, proj_rows, channels), f32),
            pltpu.VMEM((shards, proj_rows, channels), bf16),
            pltpu.VMEM((shards, proj_rows, channels), bf16),
            pltpu.VMEM((8, channels), f32),
            pltpu.VMEM((shards, 8, channels), f32),
            pltpu.VMEM((2, tok_rows + 16, channels), f32),
            dma((highs, shards)), dma((highs, shards)),
            dma((highs - 1, shards)), dma((highs - 1, shards)),
            dma((shards,)), dma((shards,)),
            dma((groups - 1,)), dma((groups,)),
            dma((shards,)), dma((shards,)),
            dma((shards,)), dma((shards,)),
            dma((2,)), dma((2,)),
        ],
        compiler_params=pltpu.CompilerParams(collective_id=1, has_side_effects=True),
    )(
        partial_rows, select_t, mid, out_grad, out_proj, branch_gate, conv_out, prior_state,
        block_diagonal(rate_gate_w), block_diagonal(input_gate_w), speed, decay_jump,
        conv_taps.astype(f32),
    )
    return (gate_grad, up_grad, down_grad, proj_grad_t, input_grad, branch_gate_grad)


def solution(mesh):
    in_specs = (
        P("sp", None),
        P("sp", None),
        P("sp", None),
        P("sp", None),
        P("sp", None, "tp"),
        P("sp", None, "tp"),
        P("sp", "tp", None),
        P("tp", None),
        P("sp", "tp"),
        P(None, "sp", "tp"),
        P(None, "sp", "tp"),
        P(None, "tp", None, None),
        P(None, "tp", None, None),
        P(None, "tp"),
        P(None, "sp", "tp"),
        P(None, None, "tp"),
    )
    out_specs = (
        P("sp", None, "tp"),
        P("sp", None, "tp"),
        P("sp", "tp", None),
        P("sp", "tp"),
        P("sp", "tp"),
        P("sp", "tp"),
    )
    return jax.shard_map(
        on_device, mesh=mesh, in_specs=in_specs, out_specs=out_specs, check_vma=False
    )
```

time: 349 us -> 136 us (0.39)
  blocking collectives: 121 us -> 0 us
  waiting for transfers between devices: 111 us -> 0 us
  Pallas kernels: 0 us -> 102 us
  other arithmetic: 40.2 us -> 7.51 us
  between operations: 15.3 us -> 0.89 us
  matrix products: 26.5 us -> 13.7 us
  starting transfers between devices: 11.6 us -> 0 us
  local copies, waits for them, and re-layouts: 22.4 us -> 10.8 us
    pallas_call x0 -> x2, Pallas kernels: none -> 102 us  [the longest x1 56.6 us: on_device(): pl.pallas_call(functools.partial(back_kernel, shards, groups), out_shape=...]
    reduce_scatter x2 -> x0, waiting for transfers between devices: 78.7 us -> none  [the longest x1 47.2 us: on_device(): lax.psum_scatter(jnp.einsum('td,tc->dc', mid_grad_b, mixed_b, preferred_e...]
    all_gather x5 -> x0, blocking collectives: 78 us -> none  [the longest x4 70.1 us: carried_in(): everything = jax.tree.map(lambda part: lax.all_gather(part, axis), x)]
    all_to_all x2 -> x0, blocking collectives: 43.2 us -> none  [the longest x1 23.8 us: on_device(): lax.all_to_all(sent_rows, 'sp', split_axis=0, concat_axis=0, tiled=True)]
    all_gather x2 -> x0, waiting for transfers between devices: 23.1 us -> none  [the longest x1 21.4 us: on_device(): lax.all_gather(got_grad, 'tp', axis=1, tiled=True)]
    select_n x16 -> x0, other arithmetic: 17.2 us -> none  [turn(): return jax.tree.map(lambda a, b: jnp.where(reached, a, b), new, before)]
    slice x99 -> x2, local copies, waits for them, and re-layouts: 13.9 us -> 3.05 us  [the longest x1 2.84 us: on_device(): expert_rows, expert_grads = (by_expert(got[0]), by_expert(got[1]))]
    all_to_all x1 -> x0, waiting for transfers between devices: 8.29 us -> none  [on_device(): lax.all_to_all(summed, 'sp', split_axis=0, concat_axis=0, tiled=True)]
  transfers between devices with their start and end apart: 7 -> 0, of which waited for: 6 -> 0; matrix products, arithmetic and copies ran while one was open for 6% -> 0% of each run, Pallas kernels for 0% -> 0%
where the time goes in v1:
time: 136 us; the launch traced here: 135 us
  Pallas kernels  102 us (75%)
  matrix products  13.7 us (10%)
  local copies, waits for them, and re-layouts  10.8 us (8%)
  other arithmetic  7.51 us (6%)
    pallas_call x1, Pallas kernels, on_device(): pl.pallas_call(functools.partial(back_kernel, shards, groups), out_shape=...  56.6 us
    pallas_call x1, Pallas kernels, on_device(): pl.pallas_call(functools.partial(front_kernel, shards, groups), out_shape...  45.6 us
    unnamed x20, local copies, waits for them, and re-layouts  5.79 us
    slice x1, local copies, waits for them, and re-layouts, on_device(): expert_rows, expert_grads = (by_expert(got[0]), by_expert(got[1]))  2.84 us

profile of v1, /device:TPU:0, one launch (start us, length us, event | category | flops | bytes accessed | tf_op | source)
XLA Modules:
  0.0 135.2 jit_solution(13983538866342753986)
XLA Ops:
  0.6 0.0 copy-start
  0.6 0.0 copy-start.1
  0.7 0.9 copy.37
  1.6 0.1 eq.64
  1.7 0.9 reduce-window.6
  2.6 0.2 slice_reduce_fusion
  2.9 0.1 eq.60
  3.0 0.1 fusion.22
  3.1 0.1 reduce_sum.30
  3.3 0.1 copy.39
  3.3 0.7 multiply_add_fusion.1
  4.0 0.2 fusion.13
  4.2 0.9 select_reduce_fusion
  5.1 1.3 fusion.3
  6.4 1.3 convert_element_type.72
  7.7 0.0 copy-done.1
  7.7 0.2 multiply_reduce_fusion
  8.0 0.4 convolution_convert_fusion.3
  8.4 1.2 pad_maximum_fusion.send
  9.5 45.6 %shard_map.199 = bf16[2,8,72,2048]{3,2,1,0:T(8,128)(2,1)} custom-call(bf16[2,8,72,512]{3,2,1,0:T(8,128)(2,1)} %pad_maximum_fusion.send), custom_call_target="tpu_custom_call" | custom-call | tf_op jit(solution)/shard_map/pallas_call | solution.py:477
  55.2 0.0 copy-start.2
  55.2 2.8 %fusion.30 = (bf16[1,8,72,2048]{3,2,1,0:T(8,128)(2,1)S(1)}, bf16[1,8,72,2048]{3,2,1,0:T(8,128)(2,1)S(1)}) fusion(bf16[2,8,72,2048]{3,2,1,0:T(8,128)(2,1)} %shard_map.199), kind=kLoop, calls=%fused_computation.59 | loop fusion | bytes 9437184 | tf_op jit(solution)/shard_map/slice | solution.py:496
  58.0 0.0 copy-done.2
  58.0 0.8 fusion.5
  58.8 0.0 copy-done
  58.8 0.0 copy-start.7
  58.9 0.8 fusion.11
  59.7 0.4 copy-done.7
  60.1 1.2 select_convert_fusion
  61.3 2.0 %fusion = bf16[1,2048,256]{2,1,0:T(8,128)(2,1)} fusion(bf16[576,2048]{1,0:T(8,128)(2,1)S(1)} %bitcast.53, bf16[576,256]{1,0:T(8,128)(2,1)S(1)} %get-tuple-element.15), kind=kOutput, calls=%fused_computation.4 | convolution fusion | flops 604504064 | bytes 3702784 | tf_op jit(solution)/shard_map/erd,erf->edf/dot_general | solution.py:522
  63.3 2.0 %fusion.1 = bf16[1,2048,256]{2,1,0:T(8,128)(2,1)} fusion(bf16[576,2048]{1,0:T(8,128)(2,1)S(1)} %bitcast.54, bf16[576,256]{1,0:T(8,128)(2,1)S(1)} %get-tuple-element.14), kind=kOutput, calls=%fused_computation.5 | convolution fusion | flops 604504064 | bytes 3702784 | tf_op jit(solution)/shard_map/erd,erf->edf/dot_general | solution.py:525
  65.3 2.1 %fusion.2 = bf16[1,256,2048]{2,1,0:T(8,128)(2,1)} fusion(bf16[576,2048]{1,0:T(8,128)(2,1)S(1)} %bitcast.50, f32[576,256]{1,0:T(8,128)S(1)} %fusion.5, f32[576,256]{1,0:T(8,128)S(1)} %fusion.11), kind=kOutput, calls=%fused_computation.6 | convolution fusion | flops 605978624 | bytes 4587520 | tf_op jit(solution)/shard_map/erf,erd->efd/dot_general | solution.py:519
  67.5 0.8 fusion.9
  68.3 0.0 copy-start.3
  68.3 0.0 copy-start.4
  68.3 2.2 %add_convert_fusion = bf16[576,2048]{1,0:T(8,128)(2,1)} fusion(f32[576,2048]{1,0:T(8,128)S(1)} %fusion.9, bf16[576,256]{1,0:T(8,128)(2,1)S(1)} %get-tuple-element.14, bf16[1,2048,256]{2,1,0:T(8,128)(2,1)S(1)} %copy-done.2), kind=kOutput, calls=%fused_computation | convolution fusion | flops 606339072 | bytes 8421376 | tf_op jit(solution)/shard_map/erf,edf->erd/dot_general | solution.py:531
  70.5 0.0 copy-start.6
  70.5 0.0 copy-start.5
  70.5 0.2 compare_reduce_fusion
  70.8 0.9 copy.40.select
  71.7 0.0 copy-done.3
  71.7 0.1 mul.136
  71.8 0.1 mul.137
  71.9 0.1 mul.132
  72.0 0.1 mul.133
  72.1 0.0 copy-done.4
  72.1 0.1 mul.130
  72.2 0.1 mul.131
  72.3 0.6 broadcast_multiply_fusion
  73.0 0.0 copy-done.6
  73.0 0.6 fusion.24.rate
  73.6 0.0 copy-done.5
  73.6 0.6 convert_element_type.89.taps
  74.2 56.6 %shard_map.200 = (f32[256,128]{1,0:T(8,128)}, bf16[192,128]{1,0:T(8,128)(2,1)}, bf16[192,128]{1,0:T(8,128)(2,1)}) custom-call(bf16[8,72,2048]{2,1,0:T(8,128)(2,1)} %bitcast.47, bf16[8,192,72]{2,1,0:T(8,128)(2,1)} %copy.40.select, bf16[192,2048]{1,0:T(8,128)(2,1)} %mid.1, bf16[192,2048]{1,0:T(8,128)(2,1)} %out_grad.1, bf16[128,2048]{1,0:T(8,128)(2,1)} %out_proj.1, ...), custom_call_target="tpu_custom_call" | custom-call | tf_op jit(solution)/shard_map/pallas_call | solution.py:554
  130.8 1.6 %copy.44 = f32[256,128]{1,0:T(8,128)} copy(f32[256,128]{1,0:T(8,128)} %get-tuple-element.27) | data formatting | bytes 262144
  132.3 1.4 %copy.45 = bf16[192,128]{1,0:T(8,128)(2,1)} copy(bf16[192,128]{1,0:T(8,128)(2,1)} %get-tuple-element.28) | data formatting | bytes 98304
  133.7 1.4 %copy.46 = bf16[192,128]{1,0:T(8,128)(2,1)} copy(bf16[192,128]{1,0:T(8,128)(2,1)} %get-tuple-element.29) | data formatting | bytes 98304
  (6 shorter events, 0.1 us)
Async XLA Ops:
  0.6 58.2 %copy-start = (bf16[1,2048,256]{2,1,0:T(8,128)(2,1)S(1)}, bf16[1,2048,256]{2,1,0:T(8,128)(2,1)}, u32[]{:S(2)}) copy-start(bf16[1,2048,256]{2,1,0:T(8,128)(2,1)} %param.20) | copy-start | bytes 3145732
  0.6 7.0 %copy-start.1 = (bf16[192,2048]{1,0:T(8,128)(2,1)S(1)}, bf16[192,2048]{1,0:T(8,128)(2,1)}, u32[]{:S(2)}) copy-start(bf16[192,2048]{1,0:T(8,128)(2,1)} %mid.1) | copy-start | bytes 2359300
  55.2 2.9 %copy-start.2 = (bf16[1,2048,256]{2,1,0:T(8,128)(2,1)S(1)}, bf16[1,2048,256]{2,1,0:T(8,128)(2,1)}, u32[]{:S(2)}) copy-start(bf16[1,2048,256]{2,1,0:T(8,128)(2,1)} %param.21) | copy-start | bytes 3145732
  58.8 1.2 copy-start.7
  68.3 3.5 %copy-start.3 = (bf16[2,2,64,64]{3,2,1,0:T(8,128)(2,1)S(1)}, bf16[2,2,64,64]{3,2,1,0:T(8,128)(2,1)}, u32[]{:S(2)}) copy-start(bf16[2,2,64,64]{3,2,1,0:T(8,128)(2,1)} %param.28) | copy-start | bytes 98308
  68.3 3.9 %copy-start.4 = (bf16[2,2,64,64]{3,2,1,0:T(8,128)(2,1)S(1)}, bf16[2,2,64,64]{3,2,1,0:T(8,128)(2,1)}, u32[]{:S(2)}) copy-start(bf16[2,2,64,64]{3,2,1,0:T(8,128)(2,1)} %param.27) | copy-start | bytes 98308
  70.5 2.5 %copy-start.6 = (f32[2,128]{1,0:T(2,128)S(1)}, f32[2,128]{1,0:T(2,128)}, u32[]{:S(2)}) copy-start(f32[2,128]{1,0:T(2,128)} %param.29) | copy-start | bytes 3076
  70.5 3.1 %copy-start.5 = (bf16[2,4,128]{2,1,0:T(4,128)(2,1)S(1)}, bf16[2,4,128]{2,1,0:T(4,128)(2,1)}, u32[]{:S(2)}) copy-start(bf16[2,4,128]{2,1,0:T(4,128)(2,1)} %param.31) | copy-start | bytes 6148

commit v2 on v1

--- a/solution.py
+++ b/solution.py
@@ -44,7 +44,10 @@
 
     lax.fori_loop(1, n, over_sp, 0)
     lax.fori_loop(1, g, over_tp, 0)
-    pl.semaphore_wait(barrier, n + g - 2)
+
+
+def greeted(n, g):
+    pl.semaphore_wait(pltpu.get_barrier_semaphore(), n + g - 2)
 
 
 def remote(src, dst, send_sem, recv_sem, axis, peer):
@@ -54,7 +57,10 @@
     )
 
 
-def front_kernel(n, g, send, got, sp_send, sp_recv, tp_send, tp_recv, own_sem):
+def front_kernel(
+    n, g, mid, out_grad, ids, weights, got_rows, got_grads, select, send, normed, ahead, named, gains,
+    sp_send, sp_recv, tp_send, tp_recv,
+):
     me, t = lax.axis_index("sp"), lax.axis_index("tp")
     low = lax.rem(t, 2)
     high = t // 2
@@ -62,65 +68,132 @@
     partner = high * 2 + 1 - low
     width = send.shape[-1]
 
-    def block(p, q):
-        return got.at[:, p, :, pl.ds(pl.multiple_of(q * width, width), width)]
-
-    def over_sp(p):
-        return remote(send.at[:, p], block(me, t), sp_send.at[p], sp_recv.at[me], "sp", p)
-
-    def from_sp(p):
-        return remote(send.at[:, p], block(p, t), sp_send.at[p], sp_recv.at[p], "sp", p)
-
-    def over_tp(kind, p, q, peer):
-        return remote(block(p, q), block(p, q), tp_send.at[kind, p], tp_recv.at[q, p], "tp", peer)
-
-    own = pltpu.make_async_copy(send.at[:, me], block(me, t), own_sem)
-    own.start()
+    both = (got_rows, got_grads)
+
+    def block(a, p, q):
+        return both[a].at[p, :, pl.ds(pl.multiple_of(q * width, width), width)]
+
+    def over_sp(a, p):
+        return remote(
+            send.at[a, p], block(a, me, t), sp_send.at[a, p], sp_recv.at[a, me], "sp", p
+        )
+
+    def from_sp(a, p):
+        return remote(
+            send.at[a, p], block(a, p, t), sp_send.at[a, p], sp_recv.at[a, p], "sp", p
+        )
+
+    def over_tp(a, kind, p, q, peer):
+        return remote(
+            block(a, p, q), block(a, p, q), tp_send.at[a, kind, p], tp_recv.at[a, q, p], "tp", peer
+        )
+
     greet(n, g)
-
-    def start(k, carry):
-        over_sp(lax.rem(me + k, n)).start()
-        return carry
-
-    lax.fori_loop(1, n, start, 0)
-    own.wait()
-
-    def spread(p):
+    rows = mid.shape[0]
+    experts, top = named.shape[0], ids.shape[0]
+    per = experts // n
+    room = select.shape[1] // per
+    f32, bf16 = jnp.float32, jnp.bfloat16
+    mine = pl.ds(pl.multiple_of(t * width, width), width)
+    piece = 16
+
+    def normal(k, carry):
+        at = pl.ds(pl.multiple_of(k * piece, piece), piece)
+        values = mid[at, :].astype(f32)
+        inv_rms = lax.rsqrt(jnp.mean(values * values, axis=1, keepdims=True) + NORM_EPSILON)
+        normed[at, :] = (mid[at, mine].astype(f32) * inv_rms).astype(bf16)
+        return carry
+
+    lax.fori_loop(0, rows // piece, normal, 0)
+    number = lax.broadcasted_iota(jnp.int32, (experts, rows), 0)
+    hit = jnp.zeros((experts, rows), f32)
+    gain = jnp.zeros((experts, rows), f32)
+    for k in range(top):
+        here = ids[k : k + 1, :] == number
+        hit = hit + jnp.where(here, 1.0, 0.0)
+        gain = gain + jnp.where(here, weights[k : k + 1, :], 0.0)
+    before = lax.broadcasted_iota(jnp.int32, (rows, rows), 0) < lax.broadcasted_iota(
+        jnp.int32, (rows, rows), 1
+    )
+    ahead[...] = jnp.dot(
+        hit.astype(bf16), jnp.where(before, 1.0, 0.0).astype(bf16), preferred_element_type=f32
+    )
+    named[...] = hit
+    gains[...] = gain
+    place = lax.broadcasted_iota(jnp.int32, (room, rows), 0).astype(f32)
+
+    def build(p):
+        picks, scales = [], []
+        for j in range(per):
+            e = p * per + j
+            pick = jnp.where(
+                (ahead[pl.ds(e, 1), :] == place) & (named[pl.ds(e, 1), :] > 0.5), 1.0, 0.0
+            )
+            picks.append(pick)
+            scales.append(jnp.sum(pick * gains[pl.ds(e, 1), :], axis=1, keepdims=True))
+        pick = picks[0] if per == 1 else jnp.concatenate(picks, axis=0)
+        scale = scales[0] if per == 1 else jnp.concatenate(scales, axis=0)
+        pick = pick.astype(bf16)
+        select[p] = pick
+        sent = jnp.dot(pick, normed[...], preferred_element_type=f32).astype(bf16)
+        grads = jnp.dot(pick, out_grad[:, mine], preferred_element_type=f32) * scale
+        return sent, grads.astype(bf16)
+
+    def spread(a, p):
         for j in range(1, highs):
-            over_tp(j, p, t, lax.rem(high + j, highs) * 2 + low).start()
-        over_tp(0, p, t, partner).start()
-
-    def forward(p):
+            over_tp(a, j, p, t, lax.rem(high + j, highs) * 2 + low).start()
+        over_tp(a, 0, p, t, partner).start()
+
+    def forward(a, p):
         for j in range(1, highs):
             q = lax.rem(high + highs - j, highs) * 2 + low
-            over_tp(j, p, q, q).wait_recv()
-            over_tp(highs - 1 + j, p, q, partner).start()
-
-    spread(me)
+            over_tp(a, j, p, q, q).wait_recv()
+            over_tp(a, highs - 1 + j, p, q, partner).start()
+
+    own_rows, own_grads = build(me)
+    got_rows[me, :, mine] = own_rows
+    got_grads[me, :, mine] = own_grads
+    greeted(n, g)
+    for a in range(2):
+        spread(a, me)
+
+    def start(k, carry):
+        p = lax.rem(me + k, n)
+        send[0, p], send[1, p] = build(p)
+        for a in range(2):
+            over_sp(a, p).start()
+        return carry
+
+    lax.fori_loop(1, n, start, 0)
 
     def step(k, carry):
         p = lax.rem(me + n - k, n)
-        from_sp(p).wait_recv()
-        spread(p)
-        forward(lax.rem(p + 1, n))
+        for a in range(2):
+            from_sp(a, p).wait_recv()
+            spread(a, p)
+        for a in range(2):
+            forward(a, lax.rem(p + 1, n))
         return carry
 
     lax.fori_loop(1, n, step, 0)
-    forward(lax.rem(me + 1, n))
+    for a in range(2):
+        forward(a, lax.rem(me + 1, n))
 
     def finish(k, carry):
         p = lax.rem(me + n - k, n)
-        for j in range(highs):
-            q = lax.rem(high + highs - j, highs) * 2 + 1 - low
-            over_tp(0, p, q, partner).wait_recv()
-        for kind in range(2 * highs - 1):
-            over_tp(kind, p, t, partner).wait_send()
+        for a in range(2):
+            for j in range(highs):
+                q = lax.rem(high + highs - j, highs) * 2 + 1 - low
+                over_tp(a, 0, p, q, partner).wait_recv()
+            for kind in range(2 * highs - 1):
+                over_tp(a, kind, p, t, partner).wait_send()
         return carry
 
     lax.fori_loop(0, n, finish, 0)
 
     def sent(k, carry):
-        over_sp(lax.rem(me + k, n)).wait_send()
+        for a in range(2):
+            over_sp(a, lax.rem(me + k, n)).wait_send()
         return carry
 
     lax.fori_loop(1, n, sent, 0)
@@ -145,6 +218,16 @@
 
 def dot_last(a, b):
     return lax.dot_general(a, b, (((1,), (1,)), ((), ())), preferred_element_type=jnp.float32)
+
+
+def dot_first(a, b):
+    return lax.dot_general(a, b, (((0,), (0,)), ((), ())), preferred_element_type=jnp.float32)
+
+
+def hand_on(a, b, c, x, y, z):
+    x[...] = a[...]
+    y[...] = b[...]
+    z[...] = c[...]
 
 
 def back_kernel(
@@ -187,6 +270,7 @@
         return remote(ready.at[p], returned.at[p], sp_send.at[p], sp_recv.at[p], "sp", p)
 
     greet(n, g)
+    greeted(n, g)
 
     def first(k, carry):
         p = lax.rem(me + k, n)
@@ -249,12 +333,12 @@
         return carry
 
     lax.fori_loop(1, n + 1, third, 0)
-    total[...] = jnp.dot(select[me], ready[me], preferred_element_type=f32)
+    total[...] = dot_first(select[me], ready[me])
 
     def fourth(k, carry):
         p = lax.rem(me + n - k, n)
         from_sp(p).wait_recv()
-        total[...] += jnp.dot(select[p], returned[p], preferred_element_type=f32)
+        total[...] += dot_first(select[p], returned[p])
         return carry
 
     lax.fori_loop(1, n, fourth, 0)
@@ -376,6 +460,7 @@
     up.wait()
     down.wait()
     reach = taps.shape[1] - 1
+    taps_full = taps[...].astype(f32)
     front = jnp.where(me > 0, padded[:, 0:edge, :], 0.0)
     end = jnp.where(me < n - 1, padded[:, edge + rows : 2 * edge + rows, :], 0.0)
     padded[:, 0:edge, :] = front
@@ -384,8 +469,8 @@
     for k in range(reach + 1):
         result = (
             result
-            + taps[0, k : k + 1, :] * padded[0, edge + reach - k : edge + reach - k + rows, :]
-            + taps[1, k : k + 1, :] * padded[1, edge - reach + k : edge - reach + k + rows, :]
+            + taps_full[0, k : k + 1, :] * padded[0, edge + reach - k : edge + reach - k + rows, :]
+            + taps_full[1, k : k + 1, :] * padded[1, edge - reach + k : edge - reach + k + rows, :]
         )
     input_o[...] = result.astype(jnp.bfloat16)
 
@@ -446,54 +531,37 @@
     top_count = expert_ids.shape[1]
     expert_room = 3 * top_count * tok_rows // (2 * experts_all)
     slot_count = experts_all * expert_room
-    mid_full = mid.astype(jnp.float32)
-    inv_rms = lax.rsqrt(jnp.mean(mid_full * mid_full, axis=1, keepdims=True) + NORM_EPSILON)
-    normed = mid_full * inv_rms
-    normed_b = normed.astype(jnp.bfloat16)
-    flat_ids = expert_ids.reshape(-1)
-    onehot = (flat_ids[:, None] == jnp.arange(experts_all, dtype=jnp.int32)[None, :]).astype(
-        jnp.int32
-    )
-    rank_ids = jnp.sum((jnp.cumsum(onehot, axis=0) - onehot) * onehot, axis=1)
-    slot_ids = (flat_ids * expert_room + rank_ids).reshape(tok_rows, top_count)
-    matches = slot_ids[None, :, :] == jnp.arange(slot_count, dtype=jnp.int32)[:, None, None]
-    select = jnp.any(matches, axis=2).astype(jnp.bfloat16)
-    slot_gate = jnp.sum(jnp.where(matches, route_weights[None, :, :], 0.0), axis=(1, 2))
     column_span = embedding_width // groups
-    offset = lax.axis_index("tp") * column_span
-    rows_source = lax.dynamic_slice_in_dim(normed_b, offset, column_span, 1)
-    grad_source = lax.dynamic_slice_in_dim(out_grad, offset, column_span, 1)
-    sent_rows = jnp.dot(select, rows_source, preferred_element_type=jnp.float32).astype(
-        jnp.bfloat16
-    )
-    dispatched_cotangent = (
-        jnp.dot(select, grad_source, preferred_element_type=jnp.float32) * slot_gate[:, None]
-    ).astype(jnp.bfloat16)
-    sending = jnp.stack([sent_rows, dispatched_cotangent]).reshape(
-        2, shards, local_experts * expert_room, column_span
-    )
+    room = local_experts * expert_room
     dma = pltpu.SemaphoreType.DMA
     vmem = pl.BlockSpec(memory_space=pltpu.VMEM)
-    got = pl.pallas_call(
+    got_rows, got_grads, select = pl.pallas_call(
         functools.partial(front_kernel, shards, groups),
-        out_shape=jax.ShapeDtypeStruct(
-            (2, shards, local_experts * expert_room, embedding_width), jnp.bfloat16
+        out_shape=(
+            jax.ShapeDtypeStruct((shards, room, embedding_width), jnp.bfloat16),
+            jax.ShapeDtypeStruct((shards, room, embedding_width), jnp.bfloat16),
+            jax.ShapeDtypeStruct((shards, room, tok_rows), jnp.bfloat16),
         ),
-        in_specs=[vmem],
-        out_specs=vmem,
+        in_specs=[vmem] * 4,
+        out_specs=(vmem,) * 3,
         scratch_shapes=[
-            dma((shards,)), dma((shards,)), dma((groups - 1, shards)), dma((groups, shards)),
-            dma(()),
+            pltpu.VMEM((2, shards, room, column_span), jnp.bfloat16),
+            pltpu.VMEM((tok_rows, column_span), jnp.bfloat16),
+            pltpu.VMEM((experts_all, tok_rows), jnp.float32),
+            pltpu.VMEM((experts_all, tok_rows), jnp.float32),
+            pltpu.VMEM((experts_all, tok_rows), jnp.float32),
+            dma((2, shards)), dma((2, shards)), dma((2, groups - 1, shards)),
+            dma((2, groups, shards)),
         ],
         compiler_params=pltpu.CompilerParams(collective_id=0, has_side_effects=True),
-    )(sending)
+    )(mid, out_grad, expert_ids.T, route_weights.T)
 
     def by_expert(block):
         return jnp.swapaxes(
             block.reshape(shards, local_experts, expert_room, embedding_width), 0, 1
         ).reshape(local_experts, shards * expert_room, embedding_width)
 
-    expert_rows, expert_grads = by_expert(got[0]), by_expert(got[1])
+    expert_rows, expert_grads = by_expert(got_rows), by_expert(got_grads)
     gate_pre = jnp.einsum(
         "erd,edf->erf", expert_rows, gate_proj, preferred_element_type=jnp.float32
     )
@@ -531,14 +599,9 @@
     partial_value = partial_value + jnp.einsum(
         "erf,edf->erd", up_delta, up_proj, preferred_element_type=jnp.float32
     )
-    room = local_experts * expert_room
     partial_rows = jnp.swapaxes(
         partial_value.reshape(local_experts, shards, expert_room, embedding_width), 0, 1
     ).reshape(shards, room, embedding_width).astype(jnp.bfloat16)
-    token_slots = jnp.arange(slot_count, dtype=jnp.int32).reshape(shards, 1, room)
-    select_t = jnp.any(
-        slot_ids[None, :, None, :] == token_slots[:, :, :, None], axis=3
-    ).astype(jnp.bfloat16)
     heads_local = rate_gate_w.shape[1]
     head_width = rate_gate_w.shape[2]
     channels = heads_local * head_width
@@ -551,7 +614,7 @@
     highs = groups // 2
     bf16, f32 = jnp.bfloat16, jnp.float32
     proj_rows = embedding_width // shards
-    proj_grad_t, input_grad, branch_gate_grad = pl.pallas_call(
+    ending = pl.pallas_call(
         functools.partial(back_kernel, shards, groups),
         out_shape=(
             jax.ShapeDtypeStruct((proj_rows, channels), f32),
@@ -589,10 +652,16 @@
         ],
         compiler_params=pltpu.CompilerParams(collective_id=1, has_side_effects=True),
     )(
-        partial_rows, select_t, mid, out_grad, out_proj, branch_gate, conv_out, prior_state,
+        partial_rows, select, mid, out_grad, out_proj, branch_gate, conv_out, prior_state,
         block_diagonal(rate_gate_w), block_diagonal(input_gate_w), speed, decay_jump,
-        conv_taps.astype(f32),
-    )
+        conv_taps,
+    )
+    proj_grad_t, input_grad, branch_gate_grad = pl.pallas_call(
+        hand_on,
+        out_shape=tuple(jax.ShapeDtypeStruct(x.shape, x.dtype) for x in ending),
+        in_specs=[vmem] * 3,
+        out_specs=(vmem,) * 3,
+    )(*ending)
     return (gate_grad, up_grad, down_grad, proj_grad_t, input_grad, branch_gate_grad)
 
 

time: 136 us -> 122 us (0.90)
  local copies, waits for them, and re-layouts: 10.8 us -> 2.12 us
  other arithmetic: 7.51 us -> 1.25 us
  Pallas kernels: 102 us -> 104 us
    unnamed x20 -> x16, local copies, waits for them, and re-layouts: 5.79 us -> 1.55 us
    slice x2 -> x0, local copies, waits for them, and re-layouts: 3.05 us -> none  [the longest x1 2.84 us: on_device(): expert_rows, expert_grads = (by_expert(got[0]), by_expert(got[1]))]
    dot_general x1, matrix products: 0.78 us -> 2.86 us  [on_device(): jnp.einsum('erd,edf->erf', expert_rows, up_proj, preferred_element_type=j...]
    another operation x4 -> x0, other arithmetic: 2.07 us -> none  [the longest x1 1.16 us: on_device(): jnp.stack([sent_rows, dispatched_cotangent])]
    convert_element_type x4 -> x0, other arithmetic: 1.95 us -> none  [the longest x1 1.3 us: on_device(): mid_full = mid.astype(jnp.float32)]
    dot_general x2 -> x0, matrix products: 1.72 us -> none  [the longest x1 1.3 us: on_device(): jnp.dot(select, grad_source, preferred_element_type=jnp.float32)]
    pallas_call x0 -> x1, Pallas kernels: none -> 1.62 us  [on_device(): pl.pallas_call(hand_on, out_shape=tuple((jax.ShapeDtypeStruct(x.shape, x....]
where the time goes in v2:
time: 122 us
  Pallas kernels  104 us (85%)
  matrix products  14 us (11%)
  local copies, waits for them, and re-layouts  2.12 us (2%)
  other arithmetic  1.25 us (1%)
    pallas_call x1, Pallas kernels, on_device(): pl.pallas_call(functools.partial(back_kernel, shards, groups), out_shape=...  55.9 us
    pallas_call x1, Pallas kernels, on_device(): pl.pallas_call(functools.partial(front_kernel, shards, groups), out_shape...  46.5 us
    dot_general x1, matrix products, on_device(): jnp.einsum('erd,edf->erf', expert_rows, up_proj, preferred_element_type=j...  2.86 us

profile of v2, /device:TPU:0, one launch (start us, length us, event | category | flops | bytes accessed | tf_op | source)
XLA Modules:
  0.0 122.2 jit_solution(17965492976127053513)
XLA Ops:
  0.6 0.0 copy-start
  0.6 46.5 %shard_map.199 = (bf16[8,72,2048]{2,1,0:T(8,128)(2,1)}, bf16[8,72,2048]{2,1,0:T(8,128)(2,1)}, bf16[8,72,192]{2,1,0:T(8,128)(2,1)}) custom-call(bf16[192,2048]{1,0:T(8,128)(2,1)} %mid.3, bf16[192,2048]{1,0:T(8,128)(2,1)} %out_grad.3, s32[2,192]{1,0:T(2,128)} %bitcast.37, f32[2,192]{1,0:T(2,128)} %bitcast.38), custom_call_target="tpu_custom_call" | custom-call | tf_op jit(solution)/shard_map/pallas_call | solution.py:538
  47.2 0.0 copy-start.6
  47.2 2.9 %fusion.4 = f32[576,256]{1,0:T(8,128)S(1)} fusion(bf16[576,2048]{1,0:T(8,128)(2,1)} %bitcast.41, bf16[1,2048,256]{2,1,0:T(8,128)(2,1)} %param.21), kind=kOutput, calls=%fused_computation.8 | convolution fusion | flops 603979776 | bytes 3997696 | tf_op jit(solution)/shard_map/erd,edf->erf/dot_general | solution.py:568
  50.0 0.0 copy-done
  50.1 0.0 copy-done.6
  50.1 0.0 copy-start.5
  50.1 0.0 copy-start.7
  50.1 0.8 fusion.10
  50.9 0.8 copy-done.5
  51.7 0.3 copy-done.7
  52.0 1.1 select_convert_fusion
  53.1 2.0 %fusion = bf16[1,2048,256]{2,1,0:T(8,128)(2,1)} fusion(bf16[576,2048]{1,0:T(8,128)(2,1)S(1)} %bitcast.43, bf16[576,256]{1,0:T(8,128)(2,1)S(1)} %get-tuple-element.25), kind=kOutput, calls=%fused_computation.4 | convolution fusion | flops 604504064 | bytes 3702784 | tf_op jit(solution)/shard_map/erd,erf->edf/dot_general | solution.py:590
  55.2 2.1 %fusion.1 = bf16[1,2048,256]{2,1,0:T(8,128)(2,1)} fusion(bf16[576,2048]{1,0:T(8,128)(2,1)S(1)} %bitcast.44, bf16[576,256]{1,0:T(8,128)(2,1)S(1)} %get-tuple-element.24), kind=kOutput, calls=%fused_computation.5 | convolution fusion | flops 604504064 | bytes 3702784 | tf_op jit(solution)/shard_map/erd,erf->edf/dot_general | solution.py:593
  57.2 2.1 %fusion.2 = bf16[1,256,2048]{2,1,0:T(8,128)(2,1)} fusion(bf16[576,2048]{1,0:T(8,128)(2,1)S(1)} %bitcast.40, f32[576,256]{1,0:T(8,128)S(1)} %fusion.4, f32[576,256]{1,0:T(8,128)S(1)} %fusion.10), kind=kOutput, calls=%fused_computation.6 | convolution fusion | flops 605978624 | bytes 4587520 | tf_op jit(solution)/shard_map/erf,erd->efd/dot_general | solution.py:587
  59.3 0.0 copy-start.1
  59.3 0.8 fusion.8
  60.1 0.4 copy-done.1
  60.5 0.0 copy-start.2
  60.5 0.0 copy-start.3
  60.5 0.0 copy-start.4
  60.5 2.2 %add_convert_fusion = bf16[576,2048]{1,0:T(8,128)(2,1)} fusion(f32[576,2048]{1,0:T(8,128)S(1)} %fusion.8, bf16[576,256]{1,0:T(8,128)(2,1)S(1)} %get-tuple-element.24, bf16[1,2048,256]{2,1,0:T(8,128)(2,1)S(1)} %copy-done.1), kind=kOutput, calls=%fused_computation | convolution fusion | flops 606339072 | bytes 8421376 | tf_op jit(solution)/shard_map/erf,edf->erd/dot_general | solution.py:599
  62.8 0.0 copy-done.2
  62.8 0.1 mul.92
  62.8 0.1 mul.93
  63.0 0.1 mul.88
  63.1 0.1 mul.89
  63.2 0.0 copy-done.3
  63.2 0.1 mul.86
  63.3 0.1 mul.87
  63.4 0.7 broadcast_multiply_fusion
  64.0 0.0 copy-done.4
  64.0 0.6 fusion.15.rate
  64.6 55.9 %shard_map.200 = (f32[256,128]{1,0:T(8,128)}, bf16[192,128]{1,0:T(8,128)(2,1)}, bf16[192,128]{1,0:T(8,128)(2,1)}) custom-call(bf16[8,72,2048]{2,1,0:T(8,128)(2,1)} %bitcast.36, bf16[8,72,192]{2,1,0:T(8,128)(2,1)} %get-tuple-element.17.select, bf16[192,2048]{1,0:T(8,128)(2,1)} %mid.3, bf16[192,2048]{1,0:T(8,128)(2,1)} %out_grad.3, ...), custom_call_target="tpu_custom_call" | custom-call | tf_op jit(solution)/shard_map/pallas_call | solution.py:617
  120.5 1.6 %shard_map.201 = (f32[256,128]{1,0:T(8,128)}, bf16[192,128]{1,0:T(8,128)(2,1)}, bf16[192,128]{1,0:T(8,128)(2,1)}) custom-call(f32[256,128]{1,0:T(8,128)} %get-tuple-element.18.a, bf16[192,128]{1,0:T(8,128)(2,1)} %get-tuple-element.19.b, bf16[192,128]{1,0:T(8,128)(2,1)} %get-tuple-element.20.c), custom_call_target="tpu_custom_call" | custom-call | tf_op jit(solution)/shard_map/pallas_call | solution.py:659
  (1 shorter events, 0.0 us)
Async XLA Ops:
  0.6 49.4 %copy-start = (bf16[1,2048,256]{2,1,0:T(8,128)(2,1)S(1)}, bf16[1,2048,256]{2,1,0:T(8,128)(2,1)}, u32[]{:S(2)}) copy-start(bf16[1,2048,256]{2,1,0:T(8,128)(2,1)} %param.20) | copy-start | bytes 3145732
  47.2 2.9 %copy-start.6 = (bf16[8,72,2048]{2,1,0:T(8,128)(2,1)S(1)}, bf16[8,72,2048]{2,1,0:T(8,128)(2,1)}, u32[]{:S(2)}) copy-start(bf16[8,72,2048]{2,1,0:T(8,128)(2,1)} %get-tuple-element.15) | copy-start | bytes 7077892
  50.1 1.7 %copy-start.5 = (bf16[8,72,2048]{2,1,0:T(8,128)(2,1)S(1)}, bf16[8,72,2048]{2,1,0:T(8,128)(2,1)}, u32[]{:S(2)}) copy-start(bf16[8,72,2048]{2,1,0:T(8,128)(2,1)} %get-tuple-element.16) | copy-start | bytes 7077892
  50.1 1.9 %copy-start.7 = (bf16[1,256,2048]{2,1,0:T(8,128)(2,1)S(1)}, bf16[1,256,2048]{2,1,0:T(8,128)(2,1)}, u32[]{:S(2)}) copy-start(bf16[1,256,2048]{2,1,0:T(8,128)(2,1)} %param.22) | copy-start | bytes 3145732
  59.3 1.2 %copy-start.1 = (bf16[1,2048,256]{2,1,0:T(8,128)(2,1)S(1)}, bf16[1,2048,256]{2,1,0:T(8,128)(2,1)}, u32[]{:S(2)}) copy-start(bf16[1,2048,256]{2,1,0:T(8,128)(2,1)} %param.21) | copy-start | bytes 3145732
  60.5 2.2 %copy-start.2 = (bf16[2,2,64,64]{3,2,1,0:T(8,128)(2,1)S(1)}, bf16[2,2,64,64]{3,2,1,0:T(8,128)(2,1)}, u32[]{:S(2)}) copy-start(bf16[2,2,64,64]{3,2,1,0:T(8,128)(2,1)} %param.28) | copy-start | bytes 98308
  60.5 2.7 %copy-start.3 = (bf16[2,2,64,64]{3,2,1,0:T(8,128)(2,1)S(1)}, bf16[2,2,64,64]{3,2,1,0:T(8,128)(2,1)}, u32[]{:S(2)}) copy-start(bf16[2,2,64,64]{3,2,1,0:T(8,128)(2,1)} %param.27) | copy-start | bytes 98308
  60.5 3.5 %copy-start.4 = (f32[2,128]{1,0:T(2,128)S(1)}, f32[2,128]{1,0:T(2,128)}, u32[]{:S(2)}) copy-start(f32[2,128]{1,0:T(2,128)} %param.29) | copy-start | bytes 3076
